TPU v7x, 256 devices: a whole 4x4x8 slice. The times are simulated.
256 devices in a mesh: sp: 32 (over z, x), tp: 8 (over y, core).
Axes of the slice: x: 4, y: 4, z: 8, core: 2. Of those that a mesh axis runs over, the one named last changes fastest.
Arguments:
- tokens: bfloat16 [2, 6144, 4096], P(None, 'sp', 'tp'), may hold values from -12 to 12
- query_weight: bfloat16 [4096, 2048], P(None, 'tp'), may hold values from -0.09375 to 0.09375
- key_weight: bfloat16 [4096, 2048], P(None, 'tp'), may hold values from -0.09375 to 0.09375
- value_weight: bfloat16 [4096, 2048], P(None, 'tp'), may hold values from -0.09375 to 0.09375
- gate_weight: bfloat16 [4096, 2048], P(None, 'tp'), may hold values from -0.09375 to 0.09375
- beta_weight: bfloat16 [4096, 16], P(None, 'tp'), may hold values from -0.09375 to 0.09375
- decay_weight: bfloat16 [4096, 16], P(None, 'tp'), may hold values from -0.09375 to 0.09375
- beta_bias: float32 [16], P('tp'), may hold values from -6 to -3
- rate_log: float32 [16], P('tp'), may hold values from -12 to -2.5
- out_gain: float32 [128], replicated, may hold values from 0.1 to 1.9
- new_query: bfloat16 [2, 16, 128], P(None, 'tp'), may hold values from -6 to 6
- new_key: bfloat16 [2, 16, 128], P(None, 'tp'), may hold values from -6 to 6
- new_value: bfloat16 [2, 16, 128], P(None, 'tp'), may hold values from -6 to 6
- new_beta: float32 [2, 16], P(None, 'tp'), may hold values from 0.1 to 0.9
- new_decay: float32 [2, 16], P(None, 'tp'), may hold values from 0.3 to 1
Outputs:
- mixed_out: bfloat16 [2, 6144, 2048], P(None, 'sp', 'tp')
- cache: bfloat16 [2, 16, 128, 128], P(None, 'tp', 'sp')
- first_out: float32 [2, 2048], P(None, 'tp')
All inputs are finite; a program needn't handle non-finite values.
Results may differ from a plain program's by a relative error of at most 0.0073.
Values may be sent and summed in bfloat16 or wider, within the bound.
A program may use at most 64 MiB of HBM per device.

v0:
```python
import jax
import jax.numpy as jnp
from jax import lax
from jax.sharding import Mesh
from jax.sharding import PartitionSpec as P

BLOCK = 64
SP = ("sp_0", "sp_1")


unit_floor = 1.0
norm_floor = 0.001
highest = lax.Precision.HIGHEST


def neutral_like(value, identity):
    return jax.tree.map(
        lambda a, e: jnp.broadcast_to(jnp.asarray(e, a.dtype), a.shape), value, identity
    )


def carried_in(value, axes, combine, identity):
    before = start = neutral_like(value, identity)
    subtotal = value
    for axis in reversed(axes):
        length, index = (lax.axis_size(axis), lax.axis_index(axis))
        pieces = jax.tree.map(lambda part: lax.all_gather(part, axis), subtotal)
        inside, subtotal = (start, start)
        for k in range(length):
            passed = k < index
            subtotal = combine(subtotal, jax.tree.map(lambda part: part[k], pieces))
            inside = jax.tree.map(lambda new, old: jnp.where(passed, new, old), subtotal, inside)
        before = combine(inside, before)
    return before


def split_up(value, dim, length):
    before, after = (value.shape[:dim], value.shape[dim + 1 :])
    return jnp.moveaxis(value.reshape(*before, length, -1, *after), dim, 0)


def summed_on_arrival(value, axis, dim):
    parts = split_up(value, dim, lax.axis_size(axis))
    arrived = lax.all_to_all(parts, axis, split_axis=0, concat_axis=0, tiled=True)
    return arrived.astype(jnp.float32).sum(axis=0)


def copy_for_each(value, axis):
    length = lax.axis_size(axis)
    return lax.all_to_all(
        jnp.broadcast_to(value[None], (length, *value.shape)), axis, 0, 0, tiled=True
    )


def over_copies(value, axis):
    everything = copy_for_each(value, axis)
    return jnp.sum(everything, axis=0)


def in_one(arrays, axis):
    ravelled, at, gathered = (jnp.concatenate([a.reshape(-1) for a in arrays]), 0, [])
    subtotal = over_copies(ravelled, axis)
    for a in arrays:
        gathered.append(subtotal[at : at + a.size].reshape(a.shape))
        at += a.size
    return tuple(gathered)


def matmul(form, left, right):
    return jnp.einsum(form, left, right, precision=highest)


def unit_rows(values):
    return values * lax.rsqrt(jnp.sum(values * values, axis=-1, keepdims=True) + unit_floor)


def head_norm(values, out_gain):
    return (
        values
        * lax.rsqrt(jnp.mean(values * values, axis=-1, keepdims=True) + norm_floor)
        * out_gain
    )


def stored(values):
    return lax.optimization_barrier(values.astype(jnp.bfloat16)).astype(jnp.float32)


def unit_lower_inverse(lower_part):
    extent = lower_part.shape[-1]
    nilpotent = -lower_part
    inverse = jnp.eye(extent, dtype=jnp.float32) + nilpotent
    for _ in range(extent.bit_length() - 2):
        nilpotent = matmul("...ij,...jk->...ik", nilpotent, nilpotent)
        inverse = inverse + matmul("...ij,...jk->...ik", nilpotent, inverse)
    return inverse


def prepare(
    query_rows,
    key_rows,
    value_rows,
    beta_in,
    decay_in,
    beta_bias,
    rate_log,
    seq_count,
    length,
    head_count,
):
    extent = query_rows.shape[-1] // head_count
    blocks = length // BLOCK

    def by_head(values):
        shaped = values.reshape(seq_count, blocks, BLOCK, head_count, extent)
        return shaped.transpose(0, 3, 1, 2, 4).reshape(
            seq_count * head_count, blocks, BLOCK, extent
        )

    def by_scalar(values):
        shaped = values.reshape(seq_count, blocks, BLOCK, head_count)
        return shaped.transpose(0, 3, 1, 2).reshape(seq_count * head_count, blocks, BLOCK)

    queries = unit_rows(by_head(query_rows))
    key_unit = unit_rows(by_head(key_rows))
    values = by_head(value_rows)
    strength = by_scalar(jax.nn.sigmoid(beta_in + beta_bias))
    decays = by_scalar(-jnp.exp(rate_log) * jax.nn.softplus(decay_in))
    return (queries, key_unit, values, strength, decays)


def block_terms(queries, key_unit, values, strength, decays):
    extent = decays.shape[-1]
    cumulative = jnp.cumsum(decays, axis=-1)
    causal = jnp.tril(jnp.ones((extent, extent), bool))
    strict = jnp.tril(jnp.ones((extent, extent), bool), -1)
    spread = cumulative[..., :, None] - cumulative[..., None, :]
    weights = jnp.where(causal, jnp.exp(jnp.where(causal, spread, 0.0)), 0.0)
    key_beta = key_unit * strength[..., None]
    lower_part = jnp.where(strict, matmul("...td,...sd->...ts", key_beta, key_unit) * weights, 0.0)
    inverse = unit_lower_inverse(lower_part)
    update = matmul("...ts,...se->...te", inverse, values * strength[..., None])
    carry_w = matmul("...ts,...sd->...td", inverse, key_beta * jnp.exp(cumulative)[..., None])
    scores = matmul("...td,...sd->...ts", queries, key_unit) * weights
    query_decay = queries * jnp.exp(cumulative)[..., None]
    last_log = cumulative[..., -1]
    key_decay = key_unit * jnp.exp(last_log[..., None] - cumulative)[..., None]
    return (update, carry_w, query_decay, scores, key_decay, last_log)


def finish_read(recall, retrieve, query_unit, key_unit, new_value, new_beta, new_decay, out_gain):
    seq_count, head_count, extent = recall.shape
    intersect = jnp.sum(key_unit * query_unit, axis=-1)
    fresh_values = new_value.astype(jnp.float32) - new_decay[..., None] * retrieve
    read_heads = new_decay[..., None] * recall + (new_beta * intersect)[..., None] * fresh_values
    return head_norm(read_heads, out_gain).reshape(seq_count, head_count * extent)


def project_rows(shard_rows, weights):
    row_count = shard_rows.shape[-1]
    flat_rows = shard_rows.reshape(-1, row_count)
    return tuple(
        (jnp.dot(flat_rows, weight, preferred_element_type=jnp.float32) for weight in weights)
    )


def shards(
    tokens,
    query_weight,
    key_weight,
    value_weight,
    gate_weight,
    beta_weight,
    decay_weight,
    beta_bias,
    rate_log,
    out_gain,
    new_query,
    new_key,
    new_value,
    new_beta,
    new_decay,
):
    seq_count, span_len, _ = tokens.shape
    head_count = rate_log.shape[0]
    weights = (query_weight, key_weight, value_weight, gate_weight, beta_weight, decay_weight)
    totals = project_rows(lax.all_gather(tokens, "tp", axis=2, tiled=True), weights)
    query_rows = stored(totals[0])
    key_rows = stored(totals[1])
    value_rows = stored(totals[2])
    gate_rows = stored(totals[3])
    prepared = prepare(
        query_rows,
        key_rows,
        value_rows,
        totals[4],
        totals[5],
        beta_bias,
        rate_log,
        seq_count,
        span_len,
        head_count,
    )
    block_data = block_terms(*prepared)
    batch_size = block_data[0].shape[0]
    extent = block_data[0].shape[-1]
    identity = jnp.broadcast_to(jnp.eye(extent, dtype=jnp.float32), (batch_size, extent, extent))

    def advance(carried, inputs):
        state_now, reach_map = carried
        u_block, w_block, qg_block, score_block, kd_block, gl_block = inputs
        fresh_values = u_block - matmul("btd,bde->bte", w_block, state_now)
        block_out = matmul("btd,bde->bte", qg_block, state_now) + matmul(
            "bts,bse->bte", score_block, fresh_values
        )
        reach_rows = qg_block - matmul("bts,bsd->btd", score_block, w_block)
        factor = jnp.exp(gl_block)[:, None, None]
        transit = factor * identity - matmul("bsd,bse->bde", kd_block, w_block)
        state_next = state_now * factor + matmul("bsd,bse->bde", kd_block, fresh_values)
        map_next = matmul("bde,bef->bdf", transit, reach_map)
        return ((state_next, map_next), (block_out, matmul("btd,bde->bte", reach_rows, reach_map)))

    inputs = tuple((jnp.moveaxis(member, 1, 0) for member in block_data))
    start_state = jnp.zeros((batch_size, extent, extent), jnp.float32)
    (local_state, local_map), (local_out, reach_all) = lax.scan(
        advance, (start_state, identity), inputs
    )

    def compose(earlier, later):
        return (
            matmul("bde,bef->bdf", later[0], earlier[0]),
            matmul("bde,bef->bdf", later[0], earlier[1]) + later[1],
        )

    prefix = carried_in(
        (local_map, local_state), SP, compose, (identity, jnp.zeros_like(local_state))
    )
    incoming = prefix[1]
    block_total = local_out + matmul("nbtd,bde->nbte", reach_all, incoming)
    blocks = span_len // BLOCK
    heads_out = block_total.reshape(blocks, seq_count, head_count, BLOCK, extent).transpose(
        1, 0, 3, 2, 4
    )
    heads_out = heads_out.reshape(seq_count, span_len, head_count, extent)
    gate_values = gate_rows.reshape(seq_count, span_len, head_count, extent)
    mixed_out = (head_norm(heads_out, out_gain) * jax.nn.silu(gate_values)).astype(jnp.bfloat16)
    mixed_out = mixed_out.reshape(seq_count, span_len, head_count * extent)
    final_state = matmul("bde,bef->bdf", local_map, incoming) + local_state
    final_cast = final_state.reshape(seq_count, head_count, extent, extent).astype(jnp.bfloat16)
    row_count = extent // lax.axis_size(SP)
    row_start = lax.axis_index(SP) * row_count
    query_unit = unit_rows(new_query.astype(jnp.float32))
    key_unit = unit_rows(new_key.astype(jnp.float32))
    is_last = lax.axis_index(SP) == lax.axis_size(SP) - 1
    own_term = jnp.where(is_last, final_cast.astype(jnp.float32), 0.0)
    cache_rows = summed_on_arrival(own_term.astype(jnp.bfloat16), SP, 2).astype(jnp.bfloat16)
    memory = lax.optimization_barrier(cache_rows).astype(jnp.float32)
    query_part = lax.dynamic_slice_in_dim(query_unit, row_start, row_count, 2)
    key_part = lax.dynamic_slice_in_dim(key_unit, row_start, row_count, 2)
    recall, retrieve = in_one(
        (matmul("shde,shd->she", memory, query_part), matmul("shde,shd->she", memory, key_part)), SP
    )
    first_out = finish_read(
        recall, retrieve, query_unit, key_unit, new_value, new_beta, new_decay, out_gain
    )
    return (mixed_out, cache_rows, first_out)


def solution(mesh):
    torus = Mesh(mesh.devices.reshape(8, 4, mesh.shape["tp"]), ("sp_0", "sp_1", "tp"))
    in_specs = (
        P(None, SP, "tp"),
        P(None, "tp"),
        P(None, "tp"),
        P(None, "tp"),
        P(None, "tp"),
        P(None, "tp"),
        P(None, "tp"),
        P("tp"),
        P("tp"),
        P(),
        P(None, "tp", None),
        P(None, "tp", None),
        P(None, "tp", None),
        P(None, "tp"),
        P(None, "tp"),
    )
    out_specs = (P(None, SP, "tp"), P(None, "tp", SP, None), P(None, "tp"))
    return jax.shard_map(
        shards, mesh=torus, in_specs=in_specs, out_specs=out_specs, check_vma=False
    )
```

profile of v0, /device:TPU:32, one launch (start us, length us, event | category | flops | bytes accessed | tf_op | source)
XLA Modules:
  0.0 294.3 jit_solution(3390538268324986770)
XLA Ops:
  9.4 33.4 %all-gather.10.cloned.1.call-done = bf16[2,192,4096]{2,1,0:T(8,128)(2,1)} async-done(((bf16[2,192,512]{2,1,0:T(8,128)(2,1)}), bf16[2,192,4096]{2,1,0:T(8,128)(2,1)}) %all-gather.10.cloned.1.call-update) | async-done | bytes 3145744 | tf_op jit(solution)/shard_map/all_gather | solution.py:187
  42.7 2.8 fusion.91
  47.5 2.9 convolution_convert_fusion.1
  52.1 2.8 fusion.50
  55.0 3.5 %convolution_convert_fusion.3 = bf16[384,256]{1,0:T(8,128)(2,1)S(1)} fusion(bf16[384,4096]{1,0:T(8,128)(2,1)} %bitcast.236, bf16[4096,256]{1,0:T(8,128)(2,1)} %param.19), kind=kOutput, calls=%fused_computation.61 | convolution fusion | flops 805404672 | bytes 5439488 | tf_op jit(solution)/shard_map/dot_general | solution.py:163
  60.2 3.6 %convolution_convert_fusion.2 = bf16[384,256]{1,0:T(8,128)(2,1)S(1)} fusion(bf16[384,4096]{1,0:T(8,128)(2,1)} %bitcast.237, bf16[4096,256]{1,0:T(8,128)(2,1)} %param.20), kind=kOutput, calls=%fused_computation.60 | convolution fusion | flops 805404672 | bytes 5439488 | tf_op jit(solution)/shard_map/dot_general | solution.py:163
  74.5 1.5 fusion.39
  76.0 29.5 %while.17 = (s32[]{:T(128)}, f32[4,128,128]{2,1,0:T(8,128)S(1)}, f32[4,128,128]{2,1,0:T(8,128)S(1)}, f32[3,4,64,128]{3,2,0,1:T(8,128)}, f32[3,4,64,128]{3,2,0,1:...) while((s32[]{:T(128)}, f32[4,128,128]{2,1,0:T(8,128)S(1)}, ...), condition=%wide.region_4.5_spmd.clone, body=%wide.region_3.4_spmd.clone.sunk | while | flops 403210240 | bytes 5445847 | solution.py:225
  80.2 1.5 convolution_add_fusion.23
  84.0 1.5 convolution_subtract_fusion.7
  90.0 1.5 convolution_add_fusion.23
  99.9 1.5 convolution_add_fusion.23
  107.1 25.9 %all-gather.12.cloned.1.call-done = f32[16,128,128]{2,1,0:T(8,128)} async-done(((f32[4,128,128]{2,1,0:T(8,128)}), f32[16,128,128]{2,1,0:T(8,128)}) %all-gather.12.cloned.1.call-update) | async-done | bytes 1048592 | tf_op jit(solution)/shard_map/all_gather | solution.py:27
  139.5 22.4 %all-gather.16.cloned.1.call-done = f32[16,128,128]{2,1,0:T(8,128)} async-done(((f32[4,128,128]{2,1,0:T(8,128)}), f32[16,128,128]{2,1,0:T(8,128)}) %all-gather.16.cloned.1.call-update) | async-done | bytes 1048592 | tf_op jit(solution)/shard_map/all_gather | solution.py:27
  168.2 4.3 %convolution_convert_fusion = bf16[384,256]{1,0:T(8,128)(2,1)} fusion(bf16[384,4096]{1,0:T(8,128)(2,1)} %bitcast.238, bf16[4096,256]{1,0:T(8,128)(2,1)} %param.21), kind=kOutput, calls=%fused_computation.58 | convolution fusion | flops 805404672 | bytes 5439488 | tf_op jit(solution)/shard_map/dot_general | solution.py:163
  173.6 31.0 %all-gather.14.cloned.1.call-done = f32[32,128,128]{2,1,0:T(8,128)} async-done(((f32[4,128,128]{2,1,0:T(8,128)}), f32[32,128,128]{2,1,0:T(8,128)}) %all-gather.14.cloned.1.call-update) | async-done | bytes 2097168 | tf_op jit(solution)/shard_map/all_gather | solution.py:27
  204.6 41.1 %all-gather.18.cloned.1.call-done = f32[32,128,128]{2,1,0:T(8,128)} async-done(((f32[4,128,128]{2,1,0:T(8,128)}), f32[32,128,128]{2,1,0:T(8,128)}) %all-gather.18.cloned.1.call-update) | async-done | bytes 2097168 | tf_op jit(solution)/shard_map/all_gather | solution.py:27
  245.6 1.5 convolution_add_fusion.20
  254.2 7.6 %all-to-all-start = ((bf16[32,2,2,4,128]{4,3,2,1,0:T(4,128)(2,1)}), bf16[32,2,2,4,128]{4,3,2,1,0:T(4,128)(2,1)S(1)}, u32[]{:S(2)}, u32[]{:S(2)}) async-start(bf16[32,2,2,4,128]{4,3,2,1,0:T(4,128)(2,1)} %bitcast.193), calls=%async_computation | async-start | bytes 262144 | tf_op jit(solution)/shard_map/all_to_all | solution.py:44
  261.8 1.6 fusion.38
  265.2 6.2 %all-to-all-done = bf16[32,2,2,4,128]{4,3,2,1,0:T(4,128)(2,1)S(1)} async-done(((bf16[32,2,2,4,128]{4,3,2,1,0:T(4,128)(2,1)}), bf16[32,2,2,4,128]{4,3,2,1,0:T(4,128)(2,1)S(1)}, u32[]{:S(2)}, u32[]{:S(2)}) %all-to-all-start) | async-done | bytes 131104 | tf_op jit(solution)/shard_map/all_to_all | solution.py:44
  272.4 4.7 %all-to-all-start.1 = ((f32[32,1,1024]{2,1,0:T(1,128)}), f32[32,1,1024]{2,1,0:T(1,128)S(1)}, u32[]{:S(2)}, u32[]{:S(2)}) async-start(f32[32,1,1024]{2,1,0:T(1,128)} %broadcast_in_dim.80), calls=%async_computation.1 | async-start | bytes 262144 | tf_op jit(solution)/shard_map/all_to_all | solution.py:50
  277.1 1.7 fusion.60
  278.9 7.9 %all-to-all-done.1 = f32[32,1,1024]{2,1,0:T(1,128)S(1)} async-done(((f32[32,1,1024]{2,1,0:T(1,128)}), f32[32,1,1024]{2,1,0:T(1,128)S(1)}, u32[]{:S(2)}, u32[]{:S(2)}) %all-to-all-start.1) | async-done | bytes 131104 | tf_op jit(solution)/shard_map/all_to_all | solution.py:50
  (195 shorter events, 67.1 us)
Async XLA Ops:
  7.2 40.4 %copy-start = (bf16[4096,256]{1,0:T(8,128)(2,1)S(1)}, bf16[4096,256]{1,0:T(8,128)(2,1)}, u32[]{:S(2)}) copy-start(bf16[4096,256]{1,0:T(8,128)(2,1)} %param.18) | copy-start | bytes 6291460
  7.2 35.6 %all-gather.10.cloned.1.call-start = ((), (), s32[]{:S(2)}) async-start(), calls=%async_computation.2 | async-start | bytes 3538944 | tf_op jit(solution)/shard_map/all_gather | solution.py:187
  7.9 125.1 %all-gather.12.cloned.1.call-start = ((), (), s32[]{:S(2)}) async-start(), calls=%async_computation.3 | async-start | bytes 1310720 | tf_op jit(solution)/shard_map/all_gather | solution.py:27
  60.2 3.8 %copy-start.20 = (f32[2,2,3,64,128]{4,3,1,0,2:T(8,128)S(1)}, f32[2,2,3,64,128]{4,3,1,0,2:T(8,128)}, u32[]{:S(2)}) copy-start(f32[2,2,3,64,128]{4,3,1,0,2:T(8,128)} %copy.189) | copy-start | bytes 1179652
  106.3 55.6 %all-gather.16.cloned.1.call-start = ((), (), s32[]{:S(2)}) async-start(), calls=%async_computation.5 | async-start | bytes 1310720 | tf_op jit(solution)/shard_map/all_gather | solution.py:27
  107.0 97.5 %all-gather.14.cloned.1.call-start = ((), (), s32[]{:S(2)}) async-start(), calls=%async_computation.4 | async-start | bytes 2359296 | tf_op jit(solution)/shard_map/all_gather | solution.py:27
  133.0 4.2 %copy-start.3 = (f32[16,128,128]{2,1,0:T(8,128)S(1)}, f32[16,128,128]{2,1,0:T(8,128)}, u32[]{:S(2)}) copy-start(f32[16,128,128]{2,1,0:T(8,128)} %all-gather.12.cloned.1.call-done) | copy-start | bytes 3145732
  139.5 106.2 %all-gather.18.cloned.1.call-start = ((), (), s32[]{:S(2)}) async-start(), calls=%async_computation.6 | async-start | bytes 2359296 | tf_op jit(solution)/shard_map/all_gather | solution.py:27
  161.9 3.5 %copy-start.22 = (f32[16,128,128]{2,1,0:T(8,128)S(1)}, f32[16,128,128]{2,1,0:T(8,128)}, u32[]{:S(2)}) copy-start(f32[16,128,128]{2,1,0:T(8,128)} %all-gather.16.cloned.1.call-done) | copy-start | bytes 3145732
  163.3 4.4 %copy-start.26 = (bf16[2,2,128]{2,1,0:T(2,128)(2,1)S(1)}, bf16[2,2,128]{2,1,0:T(2,128)(2,1)}, u32[]{:S(2)}) copy-start(bf16[2,2,128]{2,1,0:T(2,128)(2,1)} %param.27) | copy-start | bytes 3076
  163.3 4.5 %copy-start.27 = (bf16[2,2,128]{2,1,0:T(2,128)(2,1)S(1)}, bf16[2,2,128]{2,1,0:T(2,128)(2,1)}, u32[]{:S(2)}) copy-start(bf16[2,2,128]{2,1,0:T(2,128)(2,1)} %param.28) | copy-start | bytes 3076
  163.3 4.7 %copy-start.29 = (f32[2,2]{1,0:T(2,128)S(1)}, f32[2,2]{1,0:T(2,128)}, u32[]{:S(2)}) copy-start(f32[2,2]{1,0:T(2,128)} %param.30) | copy-start | bytes 52
  163.3 4.8 %copy-start.32 = (f32[128]{0:T(128)S(1)}, f32[128]{0:T(128)}, u32[]{:S(2)}) copy-start(f32[128]{0:T(128)} %param.26) | copy-start | bytes 1540
  168.1 4.3 %copy-start.8 = (f32[4,128,128]{2,1,0:T(8,128)S(1)}, f32[4,128,128]{2,1,0:T(8,128)}, u32[]{:S(2)}) copy-start(f32[4,128,128]{2,1,0:T(8,128)} %copy-done.7) | copy-start | bytes 786436
  168.1 4.3 %copy-start.10 = (f32[4,128,128]{2,1,0:T(8,128)S(1)}, f32[4,128,128]{2,1,0:T(8,128)}, u32[]{:S(2)}) copy-start(f32[4,128,128]{2,1,0:T(8,128)} %copy-done.9) | copy-start | bytes 786436
  168.2 4.3 %copy-start.12 = (f32[4,128,128]{2,1,0:T(8,128)S(1)}, f32[4,128,128]{2,1,0:T(8,128)}, u32[]{:S(2)}) copy-start(f32[4,128,128]{2,1,0:T(8,128)} %fusion.109) | copy-start | bytes 786436
  168.2 4.3 %copy-start.18 = (f32[4,128,128]{2,1,0:T(8,128)S(1)}, f32[4,128,128]{2,1,0:T(8,128)}, u32[]{:S(2)}) copy-start(f32[4,128,128]{2,1,0:T(8,128)} %copy-done.17) | copy-start | bytes 786436
  245.6 3.0 %copy-start.6 = (f32[32,128,128]{2,1,0:T(8,128)S(1)}, f32[32,128,128]{2,1,0:T(8,128)}, u32[]{:S(2)}) copy-start(f32[32,128,128]{2,1,0:T(8,128)} %all-gather.14.cloned.1.call-done) | copy-start | bytes 6291460
  245.6 4.3 %copy-start.19 = (f32[32,128,128]{2,1,0:T(8,128)S(1)}, f32[32,128,128]{2,1,0:T(8,128)}, u32[]{:S(2)}) copy-start(f32[32,128,128]{2,1,0:T(8,128)} %all-gather.18.cloned.1.call-done) | copy-start | bytes 6291460
  254.2 17.1 %all-to-all-start = ((bf16[32,2,2,4,128]{4,3,2,1,0:T(4,128)(2,1)}), bf16[32,2,2,4,128]{4,3,2,1,0:T(4,128)(2,1)S(1)}, u32[]{:S(2)}, u32[]{:S(2)}) async-start(bf16[32,2,2,4,128]{4,3,2,1,0:T(4,128)(2,1)} %bitcast.193), calls=%async_computation | async-start | bytes 262144 | tf_op jit(solution)/shard_map/all_to_all | solution.py:44
  263.9 23.0 %copy-start.30 = (bf16[2,2,128]{2,1,0:T(2,128)(2,1)S(1)}, bf16[2,2,128]{2,1,0:T(2,128)(2,1)}, u32[]{:S(2)}) copy-start(bf16[2,2,128]{2,1,0:T(2,128)(2,1)} %param.29) | copy-start | bytes 3076
  263.9 23.0 %copy-start.31 = (f32[2,2]{1,0:T(2,128)S(1)}, f32[2,2]{1,0:T(2,128)}, u32[]{:S(2)}) copy-start(f32[2,2]{1,0:T(2,128)} %param.31) | copy-start | bytes 52
  271.4 16.3 %copy-start.25 = (bf16[2,2,4,128]{3,2,1,0:T(4,128)(2,1)}, bf16[2,2,4,128]{3,2,1,0:T(4,128)(2,1)S(1)}, u32[]{:S(2)}) copy-start(bf16[2,2,4,128]{3,2,1,0:T(4,128)(2,1)S(1)} %reduce_sum.87) | copy-start | bytes 12292
  272.4 14.3 %all-to-all-start.1 = ((f32[32,1,1024]{2,1,0:T(1,128)}), f32[32,1,1024]{2,1,0:T(1,128)S(1)}, u32[]{:S(2)}, u32[]{:S(2)}) async-start(f32[32,1,1024]{2,1,0:T(1,128)} %broadcast_in_dim.80), calls=%async_computation.1 | async-start | bytes 262144 | tf_op jit(solution)/shard_map/all_to_all | solution.py:50
  (16 other events, 17.8 us)
Sparse Core Ops, SparseCore 0:
  9.8 32.8 all-gather.9
  106.4 26.5 all-gather.11
  134.8 27.0 all-gather.15
  163.5 40.9 all-gather.13
  206.2 39.4 all-gather.17
where the time goes:
time: 296 us; the launch traced here: 294 us
  waiting for transfers between devices  169 us (57%)
  matrix products  75.5 us (26%)
  between operations  14.6 us (5%)
  local copies, waits for them, and re-layouts  13.8 us (5%)
  starting transfers between devices  12.5 us (4%)
  other arithmetic  8.51 us (3%)
    all_gather x4, waiting for transfers between devices, carried_in(): pieces = jax.tree.map(lambda part: lax.all_gather(part, axis), subtotal)  120 us
    dot_general x61, matrix products, matmul(): return jnp.einsum(form, left, right, precision=highest)  55.6 us
    all_gather x1, waiting for transfers between devices, shards(): lax.all_gather(tokens, 'tp', axis=2, tiled=True)  33.4 us
    dot_general x6, matrix products, project_rows(): jnp.dot(flat_rows, weight, preferred_element_type=jnp.float32)  19.9 us
    all_to_all x1, waiting for transfers between devices, copy_for_each(): lax.all_to_all(jnp.broadcast_to(value[None], (length, *value.shape)), axi...  7.89 us
    all_to_all x1, starting transfers between devices, summed_on_arrival(): lax.all_to_all(parts, axis, split_axis=0, concat_axis=0, tiled=True)  7.57 us
    all_to_all x1, waiting for transfers between devices, summed_on_arrival(): lax.all_to_all(parts, axis, split_axis=0, concat_axis=0, tiled=True)  6.16 us
  transfers between devices with their start and end apart: 7, of which 7 were waited for; matrix products, arithmetic and copies ran while one was open for 7% of the time, Pallas kernels for 0%

commit v1 on v0

v1 whole, which is shorter than its diff:
```python
import jax
import jax.numpy as jnp
from jax import lax
from jax.experimental import pallas as pl
from jax.experimental.pallas import tpu as pltpu
from jax.sharding import Mesh
from jax.sharding import PartitionSpec as P

MESH = pl.DeviceIdType.MESH
F32 = jnp.float32
BF = jnp.bfloat16
NZ, NX, NY, NC = 8, 4, 4, 2
L = 192
HALF = L // 2
E = 128
KC = 512
D = 4096
PAD = 16


def dot(a, b):
    return jnp.dot(a, b, preferred_element_type=F32)


def dot_nt(a, b):
    return lax.dot_general(a, b, (((1,), (1,)), ((), ())), preferred_element_type=F32)


def dot_tn(a, b):
    return lax.dot_general(a, b, (((0,), (0,)), ((), ())), preferred_element_type=F32)


def split3(x):
    hi = x.astype(BF)
    rest = x - hi.astype(F32)
    mid = rest.astype(BF)
    low = (rest - mid.astype(F32)).astype(BF)
    return hi, mid, low


def compose(later, earlier):
    al, rl, sl = later
    ae, re, se = earlier
    prod = dot(rl.astype(BF), jnp.concatenate([re, se], axis=1).astype(BF))
    r = al * re + ae * rl - prod[:, :E]
    s = al * se + sl - prod[:, E:]
    return al * ae, r, s


def apply_map(m, state):
    a, r, s = m
    return a * state - dot(r.astype(BF), state.astype(BF)) + s


def write_map(ref, a, r, s):
    ref[0, 0:E, :] = r.astype(BF)
    hi, mid, low = split3(a)
    row = lax.broadcasted_iota(jnp.int32, (PAD, E), 0)
    tail = jnp.where(
        row == 0,
        hi.astype(F32),
        jnp.where(row == 1, mid.astype(F32), jnp.where(row == 2, low.astype(F32), 0.0)),
    )
    ref[0, E : E + PAD, :] = tail.astype(BF)
    ref[1, 0:E, :] = s.astype(BF)


def read_map(ref):
    tail = ref[0, E : E + PAD, :].astype(F32)
    a = jnp.sum(tail, axis=0, keepdims=True)
    return a, ref[0, 0:E, :].astype(F32), ref[1, 0:E, :].astype(F32)


def kernel(
    bias_ref,
    rate_ref,
    nbeta_ref,
    ndecay_ref,
    tok_ref,
    wq_ref,
    wk_ref,
    wv_ref,
    wg_ref,
    wbd_ref,
    gain_ref,
    nq_ref,
    nk_ref,
    nv_ref,
    out_ref,
    cache_ref,
    first_ref,
    xbuf,
    wbuf,
    pj,
    lo,
    reach,
    msg,
    xin,
    zin,
    ret,
    pin,
    side,
    sin,
    wsem,
    tsem,
    ys_sem,
    yr_sem,
    fs_sem,
    fr_sem,
    ps_sem,
    pr_sem,
    xs_sem,
    xr_sem,
    zs_sem,
    zr_sem,
    rs_sem,
    rr_sem,
    ss_sem,
    sr_sem,
):
    z, x, y, c = (lax.axis_index(n) for n in ("z", "x", "y", "c"))
    yu, yd = lax.rem(y + 1, NY), lax.rem(y + NY - 1, NY)
    yf = lax.rem(y + 2, NY)
    zu, zd = lax.rem(z + 1, NZ), lax.rem(z + NZ - 1, NZ)
    other = 1 - c

    def cols(yy, cc):
        return pl.ds(pl.multiple_of((yy * NC + cc) * KC, KC), KC)

    wcopies = []
    for i, w in enumerate((wq_ref, wk_ref, wv_ref, wg_ref)):
        cp = pltpu.make_async_copy(w, wbuf.at[i], wsem.at[i])
        wcopies.append(cp)
    tcopies = []
    for s in range(2):
        cp = pltpu.make_async_copy(tok_ref.at[s], xbuf.at[s, :, cols(y, c)], tsem.at[s])
        cp.start()
        tcopies.append(cp)
    for cp in wcopies:
        cp.start()

    barrier = pltpu.get_barrier_semaphore()
    partners = [{"y": yu}, {"y": yd}, {"c": other}, {"z": zu}, {"z": zd}]
    partners += [{"x": lax.rem(x + d, NX)} for d in (1, 2, 3)]
    for p in partners:
        pl.semaphore_signal(barrier, inc=1, device_id=p, device_id_type=MESH)
    pl.semaphore_wait(barrier, len(partners))

    def ycopy(s, half, direction):
        part = xbuf.at[s, pl.ds(half * HALF, HALF), cols(y, c)]
        return pltpu.make_async_remote_copy(
            src_ref=part,
            dst_ref=part,
            send_sem=ys_sem.at[s, half, direction],
            recv_sem=yr_sem.at[s, half, direction],
            device_id={"y": yu if direction == 0 else yd},
            device_id_type=MESH,
        )

    def yarrive(s, half, direction):
        part = xbuf.at[s, pl.ds(half * HALF, HALF), cols(yd if direction == 0 else yu, c)]
        return pltpu.make_async_remote_copy(
            src_ref=part,
            dst_ref=part,
            send_sem=ys_sem.at[s, half, direction],
            recv_sem=yr_sem.at[s, half, direction],
            device_id={"y": yu if direction == 0 else yd},
            device_id_type=MESH,
        )

    def fcopy(s, direction):
        part = xbuf.at[s, pl.ds(direction * HALF, HALF), cols(yd if direction == 0 else yu, c)]
        return pltpu.make_async_remote_copy(
            src_ref=part,
            dst_ref=part,
            send_sem=fs_sem.at[s, direction],
            recv_sem=fr_sem.at[s, direction],
            device_id={"y": yu if direction == 0 else yd},
            device_id_type=MESH,
        )

    def farrive(s, direction):
        part = xbuf.at[s, pl.ds(direction * HALF, HALF), cols(yf, c)]
        return pltpu.make_async_remote_copy(
            src_ref=part,
            dst_ref=part,
            send_sem=fs_sem.at[s, direction],
            recv_sem=fr_sem.at[s, direction],
            device_id={"y": yu if direction == 0 else yd},
            device_id_type=MESH,
        )

    def pcopy(s, k, cc):
        part = xbuf.at[s, :, cols((y, yd, yu, yf)[k], cc)]
        return pltpu.make_async_remote_copy(
            src_ref=part,
            dst_ref=part,
            send_sem=ps_sem.at[s, k],
            recv_sem=pr_sem.at[s, k],
            device_id={"c": other},
            device_id_type=MESH,
        )

    def send_own(s):
        tcopies[s].wait()
        ycopy(s, 0, 0).start()
        ycopy(s, 1, 1).start()
        ycopy(s, 1, 0).start()
        ycopy(s, 0, 1).start()
        pcopy(s, 0, c).start()

    def forward(s):
        yarrive(s, 0, 0).wait_recv()
        fcopy(s, 0).start()
        yarrive(s, 1, 1).wait_recv()
        fcopy(s, 1).start()

    def finish_gather(s):
        yarrive(s, 1, 0).wait_recv()
        pcopy(s, 1, c).start()
        yarrive(s, 0, 1).wait_recv()
        pcopy(s, 2, c).start()
        farrive(s, 0).wait_recv()
        farrive(s, 1).wait_recv()
        pcopy(s, 3, c).start()
        for k in range(4):
            pcopy(s, k, other).wait_recv()

    it = lax.broadcasted_iota(jnp.int32, (L, L), 0)
    js = lax.broadcasted_iota(jnp.int32, (L, L), 1)
    lower = it >= js
    strict = it > js

    def project(s):
        def body(i, carry):
            pj[s, i] = dot(xbuf[s], wbuf[i]).astype(BF)
            return carry

        lax.fori_loop(0, 4, body, 0)

    def local_terms(s):
        bd = dot_nt(xbuf[s], wbd_ref[...])
        lane = lax.broadcasted_iota(jnp.int32, (L, PAD), 1)
        bias = jnp.where(lane == 0, bias_ref[0], jnp.where(lane == 1, bias_ref[1], 0.0))
        rate = jnp.where(lane == 2, rate_ref[0], jnp.where(lane == 3, rate_ref[1], 0.0))
        beta = jax.nn.sigmoid(bd + bias)
        soft = jnp.maximum(bd, 0.0) + jnp.log1p(jnp.exp(-jnp.abs(bd)))
        g = -jnp.exp(rate) * soft
        tri = jnp.where(lower, 1.0, 0.0).astype(BF)
        cum = sum(dot(tri, part) for part in split3(g))
        heads = range(2)
        qs = [pj[s, 0, :, h * E : (h + 1) * E] for h in heads]
        ks = [pj[s, 1, :, h * E : (h + 1) * E] for h in heads]
        vs = [pj[s, 2, :, h * E : (h + 1) * E] for h in heads]

        def scale(v):
            v = v.astype(F32)
            return lax.rsqrt(jnp.sum(v * v, axis=1, keepdims=True) + 1.0)

        rq = [scale(v) for v in qs]
        rk = [scale(v) for v in ks]
        pack = jnp.where(lane == 0, rk[0], jnp.where(lane == 1, rk[1], cum))
        eye = jnp.where(
            lax.broadcasted_iota(jnp.int32, (PAD, PAD), 0)
            == lax.broadcasted_iota(jnp.int32, (PAD, PAD), 1),
            1.0,
            0.0,
        ).astype(BF)
        rows = sum(dot_nt(eye, part) for part in split3(pack))
        amats, scores, cumc, betac = [], [], [], []
        for h in heads:
            cc = cum[:, 2 + h : 3 + h]
            bc = beta[:, h : h + 1]
            cumc.append(cc)
            betac.append(bc)
            rrow = rows[h : h + 1, :]
            crow = rows[2 + h : 3 + h, :]
            decay = jnp.exp(jnp.where(lower, cc - crow, 0.0)) * rrow
            kk = dot_nt(ks[h], ks[h])
            qk = dot_nt(qs[h], ks[h])
            amats.append(jnp.where(strict, kk * (bc * rk[h]) * decay, 0.0))
            scores.append(jnp.where(lower, qk * rq[h] * decay, 0.0).astype(BF))

        def level_mask(bit):
            return ((it >> (bit + 1)) == (js >> (bit + 1))) & ((it >> bit) != (js >> bit))

        m0 = level_mask(0)
        invs = [-jnp.where(m0, a, 0.0) for a in amats]
        for bit in range(1, 8):
            m = level_mask(bit)
            for h in heads:
                off = jnp.where(m, amats[h], 0.0)
                inv = invs[h]
                ib = inv.astype(BF)
                yy = off + dot(off.astype(BF), ib)
                invs[h] = inv - yy - dot(ib, yy.astype(BF))
        for h in heads:
            b = 2 * s + h
            kf = ks[h].astype(F32)
            ecum = jnp.exp(cumc[h])
            rhs = jnp.concatenate(
                [kf * (betac[h] * rk[h] * ecum), vs[h].astype(F32) * betac[h]], axis=1
            )
            sol = rhs + dot(invs[h].astype(BF), rhs.astype(BF))
            sb = sol.astype(BF)
            last = cumc[h][L - 1 : L, :]
            kd = kf * (rk[h] * jnp.exp(last - cumc[h]))
            rs = dot_tn(kd.astype(BF), sb)
            sx = dot(scores[h], sb)
            a = jnp.broadcast_to(jnp.exp(last), (1, E))
            write_map(msg.at[b], a, rs[:, :E], rs[:, E:])
            lo[b] = sx[:, E:]
            qd = qs[h].astype(F32) * (rq[h] * ecum)
            reach[b] = (qd - sx[:, :E]).astype(BF)

    def xcopy(b, src_x):
        return pltpu.make_async_remote_copy(
            src_ref=msg.at[b],
            dst_ref=xin.at[src_x],
            send_sem=xs_sem.at[b],
            recv_sem=xr_sem.at[src_x],
            device_id={"x": b},
            device_id_type=MESH,
        )

    def xlocal(b):
        return pltpu.make_async_copy(msg.at[b], xin.at[b], xs_sem.at[b])

    def xsend(b):
        @pl.when(x != b)
        def _():
            xcopy(b, x).start()

        @pl.when(x == b)
        def _():
            xlocal(b).start()

    send_own(0)
    forward(0)
    send_own(1)
    finish_gather(0)
    for cp in wcopies:
        cp.wait()
    project(0)
    forward(1)
    local_terms(0)
    xsend(0)
    xsend(1)
    finish_gather(1)
    project(1)
    local_terms(1)
    xsend(2)
    xsend(3)

    for j in range(NX):

        @pl.when(x != j)
        def _():
            xcopy(j, j).wait_recv()

        @pl.when(x == j)
        def _():
            xlocal(j).wait()

    maps = [read_map(xin.at[j]) for j in range(NX)]
    m10 = compose(maps[1], maps[0])
    m32 = compose(maps[3], maps[2])
    total = compose(m32, m10)
    write_map(zin.at[z], *total)

    def zslot(step, direction):
        if direction == 0:
            return lax.rem(z + NZ - (step - 1), NZ)
        return lax.rem(z + (step - 1), NZ)

    def zcopy(step, piece, direction, slot):
        part = zin.at[slot, piece]
        return pltpu.make_async_remote_copy(
            src_ref=part,
            dst_ref=part,
            send_sem=zs_sem.at[step - 1, piece, direction],
            recv_sem=zr_sem.at[step - 1, piece, direction],
            device_id={"z": zu if direction == 0 else zd},
            device_id_type=MESH,
        )

    for step in range(1, 5):
        for piece in range(2):
            for direction in range(2):
                if direction == 1 and step > 3:
                    continue
                slot = zslot(step, direction)
                if step > 1:
                    zcopy(step - 1, piece, direction, slot).wait_recv()
                zcopy(step, piece, direction, slot).start()
    m210 = compose(maps[2], m10)
    for piece in range(2):
        zcopy(3, piece, 1, zslot(4, 1)).wait_recv()
        zcopy(4, piece, 0, zslot(5, 0)).wait_recv()

    state = jnp.zeros((E, E), F32)
    here = state
    for k in range(NZ):
        here = jnp.where(z == k, state, here)
        m = read_map(zin.at[k])
        state = m[2] if k == 0 else apply_map(m, state)
    starts = [here] + [apply_map(m, here) for m in (maps[0], m10, m210)]

    def rcopy(j, b):
        return pltpu.make_async_remote_copy(
            src_ref=ret.at[j],
            dst_ref=pin.at[b],
            send_sem=rs_sem.at[j],
            recv_sem=rr_sem.at[b],
            device_id={"x": j},
            device_id_type=MESH,
        )

    def rlocal(j):
        return pltpu.make_async_copy(ret.at[j], pin.at[j], rs_sem.at[j])

    def scopy(j, b):
        return pltpu.make_async_remote_copy(
            src_ref=side.at[j],
            dst_ref=sin.at[b],
            send_sem=ss_sem.at[j],
            recv_sem=sr_sem.at[b],
            device_id={"x": j},
            device_id_type=MESH,
        )

    def slocal(j):
        return pltpu.make_async_copy(side.at[j], sin.at[j], ss_sem.at[j])

    for j in range(NX):
        ret[j] = starts[j].astype(BF)

        @pl.when(x != j)
        def _():
            rcopy(j, x).start()

        @pl.when(x == j)
        def _():
            rlocal(j).start()

    memory = state.astype(BF)

    def pick(ref):
        row = ref[0, 0:1, :].astype(F32)
        for b in range(1, 4):
            row = jnp.where(x == b, ref[b // 2, b % 2 : b % 2 + 1, :].astype(F32), row)
        return row

    def pick_scalar(ref):
        value = ref[0, 0]
        for b in range(1, 4):
            value = jnp.where(x == b, ref[b // 2, b % 2], value)
        return value

    def unit(v):
        return v * lax.rsqrt(jnp.sum(v * v, axis=1, keepdims=True) + 1.0)

    qn, kn, nv = unit(pick(nq_ref)), unit(pick(nk_ref)), pick(nv_ref)
    nbeta, ndecay = pick_scalar(nbeta_ref), pick_scalar(ndecay_ref)
    row8 = lax.broadcasted_iota(jnp.int32, (PAD, E), 0)
    probe = jnp.where(row8 == 0, qn, jnp.where(row8 == 1, kn, 0.0))
    seen = sum(dot(part, memory) for part in split3(probe))
    recall, retrieve = seen[0:1, :], seen[1:2, :]
    intersect = jnp.sum(kn * qn, axis=1, keepdims=True)
    fresh = nv - ndecay * retrieve
    read = ndecay * recall + (nbeta * intersect) * fresh
    gain = gain_ref[...]
    first = read * lax.rsqrt(jnp.mean(read * read, axis=1, keepdims=True) + 0.001) * gain

    memf = memory.astype(F32)
    mine = memf[0:16, :]
    for k in range(1, NZ):
        mine = jnp.where(z == k, memf[16 * k : 16 * k + 16, :], mine)
    for j in range(NX):
        side[j, 0:4, :] = mine[4 * j : 4 * j + 4, :]
        side[j, 4:8, :] = jnp.broadcast_to(first, (4, E))

        @pl.when(x != j)
        def _():
            scopy(j, x).start()

        @pl.when(x == j)
        def _():
            slocal(j).start()

    for b in range(4):

        @pl.when(x != b)
        def _():
            rcopy(b, b).wait_recv()

        @pl.when(x == b)
        def _():
            rlocal(b).wait()

    for b in range(4):
        s, h = b // 2, b % 2
        o = lo[b] + dot(reach[b], pin[b])
        gate = pj[s, 3, :, h * E : (h + 1) * E].astype(F32)
        norm = lax.rsqrt(jnp.mean(o * o, axis=1, keepdims=True) + 0.001)
        out_ref[s, :, h * E : (h + 1) * E] = (
            o * norm * gain * (gate * jax.nn.sigmoid(gate))
        ).astype(BF)

    for b in range(4):

        @pl.when(x != b)
        def _():
            scopy(b, b).wait_recv()

        @pl.when(x == b)
        def _():
            slocal(b).wait()

    for b in range(4):
        s, h = b // 2, b % 2
        cache_ref[s, h] = sin[b, 0:4, :].astype(BF)
        first_ref[s : s + 1, h * E : (h + 1) * E] = sin[b, 4:5, :]

    for s in range(2):
        for half in range(2):
            for direction in range(2):
                ycopy(s, half, direction).wait_send()
        for direction in range(2):
            fcopy(s, direction).wait_send()
        for k in range(4):
            pcopy(s, k, c).wait_send()
    for j in range(NX):

        @pl.when(x != j)
        def _():
            xcopy(j, x).wait_send()
            rcopy(j, x).wait_send()
            scopy(j, x).wait_send()

    for step in range(1, 5):
        for piece in range(2):
            for direction in range(2):
                if direction == 1 and step > 3:
                    continue
                zcopy(step, piece, direction, zslot(step, direction)).wait_send()


def shards(
    tokens,
    query_weight,
    key_weight,
    value_weight,
    gate_weight,
    beta_weight,
    decay_weight,
    beta_bias,
    rate_log,
    out_gain,
    new_query,
    new_key,
    new_value,
    new_beta,
    new_decay,
):
    wbd = jnp.concatenate(
        [beta_weight.T, decay_weight.T, jnp.zeros((PAD - 4, D), BF)], axis=0
    )
    smem = pl.BlockSpec(memory_space=pltpu.SMEM)
    vmem = pl.BlockSpec(memory_space=pltpu.VMEM)
    hbm = pl.BlockSpec(memory_space=pl.ANY)
    dma = pltpu.SemaphoreType.DMA
    out = pl.pallas_call(
        kernel,
        out_shape=(
            jax.ShapeDtypeStruct((2, L, 2 * E), BF),
            jax.ShapeDtypeStruct((2, 2, 4, E), BF),
            jax.ShapeDtypeStruct((2, 2 * E), F32),
        ),
        in_specs=[smem] * 4 + [hbm] * 5 + [vmem] * 5,
        out_specs=(vmem, vmem, vmem),
        scratch_shapes=[
            pltpu.VMEM((2, L, D), BF),
            pltpu.VMEM((4, D, 2 * E), BF),
            pltpu.VMEM((2, 4, L, 2 * E), BF),
            pltpu.VMEM((4, L, E), F32),
            pltpu.VMEM((4, L, E), BF),
            pltpu.VMEM((4, 2, E + PAD, E), BF),
            pltpu.VMEM((4, 2, E + PAD, E), BF),
            pltpu.VMEM((NZ, 2, E + PAD, E), BF),
            pltpu.VMEM((4, E, E), BF),
            pltpu.VMEM((4, E, E), BF),
            pltpu.VMEM((4, 8, E), F32),
            pltpu.VMEM((4, 8, E), F32),
            dma((4,)),
            dma((2,)),
            dma((2, 2, 2)),
            dma((2, 2, 2)),
            dma((2, 2)),
            dma((2, 2)),
            dma((2, 4)),
            dma((2, 4)),
            dma((4,)),
            dma((4,)),
            dma((4, 2, 2)),
            dma((4, 2, 2)),
            dma((4,)),
            dma((4,)),
            dma((4,)),
            dma((4,)),
        ],
        compiler_params=pltpu.CompilerParams(
            collective_id=0, has_side_effects=True, vmem_limit_bytes=60 * 1024 * 1024
        ),
        name="delta_all",
    )(
        beta_bias,
        rate_log,
        new_beta,
        new_decay,
        tokens,
        query_weight,
        key_weight,
        value_weight,
        gate_weight,
        wbd,
        out_gain.reshape(1, E),
        new_query,
        new_key,
        new_value,
    )
    return out


def solution(mesh):
    torus = Mesh(mesh.devices.reshape(NZ, NX, NY, NC), ("z", "x", "y", "c"))
    sp, tp = ("z", "x"), ("y", "c")
    in_specs = (
        P(None, sp, tp),
        P(None, tp),
        P(None, tp),
        P(None, tp),
        P(None, tp),
        P(None, tp),
        P(None, tp),
        P(tp),
        P(tp),
        P(),
        P(None, tp, None),
        P(None, tp, None),
        P(None, tp, None),
        P(None, tp),
        P(None, tp),
    )
    out_specs = (P(None, sp, tp), P(None, tp, sp, None), P(None, tp))
    return jax.shard_map(
        shards, mesh=torus, in_specs=in_specs, out_specs=out_specs, check_vma=False
    )
```

time: 296 us -> 67.9 us (0.23)
  waiting for transfers between devices: 169 us -> 0 us
  matrix products: 75.5 us -> 0 us
  Pallas kernels: 0 us -> 61.2 us
  between operations: 14.6 us -> 0.65 us
  starting transfers between devices: 12.5 us -> 0 us
  local copies, waits for them, and re-layouts: 13.8 us -> 4.19 us
  other arithmetic: 8.51 us -> 1.47 us
    all_gather x5 -> x0, waiting for transfers between devices: 154 us -> none  [the longest x4 120 us: carried_in(): pieces = jax.tree.map(lambda part: lax.all_gather(part, axis), subtotal)]
    dot_general x67 -> x0, matrix products: 75.5 us -> none  [the longest x61 55.6 us: matmul(): return jnp.einsum(form, left, right, precision=highest)]
    pallas_call x0 -> x1, Pallas kernels: none -> 61.2 us  [shards(): pl.pallas_call(kernel, out_shape=(jax.ShapeDtypeStruct((2, L, 2 * E), BF)...]
    all_to_all x2 -> x0, waiting for transfers between devices: 14 us -> none  [the longest x1 7.89 us: copy_for_each(): lax.all_to_all(jnp.broadcast_to(value[None], (length, *value.shape)), axi...]
    all_to_all x2 -> x0, starting transfers between devices: 12.3 us -> none  [the longest x1 7.57 us: summed_on_arrival(): lax.all_to_all(parts, axis, split_axis=0, concat_axis=0, tiled=True)]
  transfers between devices with their start and end apart: 7 -> 0, of which waited for: 7 -> 0; matrix products, arithmetic and copies ran while one was open for 7% -> 0% of each run, Pallas kernels for 0% -> 0%
where the time goes in v1:
time: 67.9 us; the launch traced here: 67.6 us
  Pallas kernels  61.2 us (90%)
  local copies, waits for them, and re-layouts  4.19 us (6%)
  other arithmetic  1.47 us (2%)
    pallas_call x1, Pallas kernels, shards(): pl.pallas_call(kernel, out_shape=(jax.ShapeDtypeStruct((2, L, 2 * E), BF)...  61.2 us
    unnamed x3, local copies, waits for them, and re-layouts  4.11 us
    concatenate x1, other arithmetic, shards(): jnp.concatenate([beta_weight.T, decay_weight.T, jnp.zeros((PAD - 4, D), B...  1.47 us

profile of v1, /device:TPU:32, one launch (start us, length us, event | category | flops | bytes accessed | tf_op | source)
XLA Modules:
  0.0 67.6 jit_solution(14960000972695392283)
XLA Ops:
  0.6 0.1 pad.2.clone
  0.7 1.5 %maximum_maximum_fusion.wbd_ref = bf16[16,4096]{1,0:T(8,128)(2,1)} fusion(bf16[2,4096]{1,0:T(2,128)(2,1)} %bitcast.3, bf16[2,4096]{1,0:T(2,128)(2,1)} %bitcast.4, bf16[16]{0:T(256)(128)(2,1)S(1)} %pad.2.clone), kind=kLoop, calls=%fused_computation | loop fusion | flops 393216 | bytes 163872 | tf_op jit(solution)/shard_map/concatenate | solution.py:566
  2.2 61.2 %delta_all.1 = (bf16[2,192,256]{2,1,0:T(8,128)(2,1)}, bf16[2,2,4,128]{3,2,1,0:T(4,128)(2,1)}, f32[2,256]{1,0:T(2,128)}) custom-call(f32[2]{0:T(128)} %bias_ref.1, f32[2]{0:T(128)} %rate_ref.1, f32[2,2]{1,0:T(2,128)} %nbeta_ref.1, f32[2,2]{1,0:T(2,128)} %ndecay_ref.1, bf16[2,192,512]{2,1,0:T(8,128)(2,1)} %tok_ref.1, bf16[4096,256]{1,0:T(8,128)(2,1)} %wq_ref.1, ...), custom_call_target="tpu_custom_call" | custom-call | tf_op jit(solution)/shard_map/delta_all/pallas_call | solution.py:573
  63.4 1.6 %copy.21 = bf16[2,192,256]{2,1,0:T(8,128)(2,1)} copy(bf16[2,192,256]{2,1,0:T(8,128)(2,1)} %get-tuple-element.6) | data formatting | bytes 393216
  65.1 1.3 %copy.22 = bf16[2,2,4,128]{3,2,1,0:T(4,128)(2,1)} copy(bf16[2,2,4,128]{3,2,1,0:T(4,128)(2,1)} %get-tuple-element.7) | data formatting | bytes 8192
  66.3 1.2 %copy.23 = f32[2,256]{1,0:T(2,128)} copy(f32[2,256]{1,0:T(2,128)} %get-tuple-element.8) | data formatting | bytes 4096
  (1 shorter events, 0.0 us)

commit v2 on v1

--- a/solution.py
+++ b/solution.py
@@ -81,7 +81,8 @@
     wk_ref,
     wv_ref,
     wg_ref,
-    wbd_ref,
+    wb_ref,
+    wd_ref,
     gain_ref,
     nq_ref,
     nk_ref,
@@ -92,8 +93,11 @@
     xbuf,
     wbuf,
     pj,
+    acc,
+    wbd,
     lo,
     reach,
+    sols,
     msg,
     xin,
     zin,
@@ -139,6 +143,10 @@
     for cp in wcopies:
         cp.start()
 
+    wbd[...] = jnp.concatenate(
+        [wb_ref[...].astype(F32), wd_ref[...].astype(F32), jnp.zeros((PAD - 4, D), F32)], axis=0
+    ).astype(BF)
+
     barrier = pltpu.get_barrier_semaphore()
     partners = [{"y": yu}, {"y": yd}, {"c": other}, {"z": zu}, {"z": zd}]
     partners += [{"x": lax.rem(x + d, NX)} for d in (1, 2, 3)]
@@ -215,31 +223,55 @@
         yarrive(s, 1, 1).wait_recv()
         fcopy(s, 1).start()
 
-    def finish_gather(s):
+    def finish_near(s):
         yarrive(s, 1, 0).wait_recv()
         pcopy(s, 1, c).start()
         yarrive(s, 0, 1).wait_recv()
         pcopy(s, 2, c).start()
+        for k in range(3):
+            pcopy(s, k, other).wait_recv()
+
+    def finish_far(s):
         farrive(s, 0).wait_recv()
         farrive(s, 1).wait_recv()
         pcopy(s, 3, c).start()
-        for k in range(4):
-            pcopy(s, k, other).wait_recv()
+        pcopy(s, 3, other).wait_recv()
 
     it = lax.broadcasted_iota(jnp.int32, (L, L), 0)
     js = lax.broadcasted_iota(jnp.int32, (L, L), 1)
     lower = it >= js
     strict = it > js
 
-    def project(s):
-        def body(i, carry):
+    def project(s, which):
+        for i in which:
             pj[s, i] = dot(xbuf[s], wbuf[i]).astype(BF)
-            return carry
-
-        lax.fori_loop(0, 4, body, 0)
-
-    def local_terms(s):
-        bd = dot_nt(xbuf[s], wbd_ref[...])
+
+    def small(s):
+        return dot_nt(xbuf[s], wbd[...])
+
+    def chip(yy):
+        return pl.ds(pl.multiple_of(yy * NC * KC, NC * KC), NC * KC)
+
+    def near(s):
+        for n, i in enumerate((1, 2)):
+            acc[n] = sum(dot(xbuf[s, :, chip(q)], wbuf[i, chip(q), :]) for q in (y, yd, yu))
+        return sum(dot_nt(xbuf[s, :, chip(q)], wbd[:, chip(q)]) for q in (y, yd, yu))
+
+    def far(s, part):
+        for n, i in enumerate((1, 2)):
+            pj[s, i] = (acc[n] + dot(xbuf[s, :, chip(yf)], wbuf[i, chip(yf), :])).astype(BF)
+        return part + dot_nt(xbuf[s, :, chip(yf)], wbd[:, chip(yf)])
+
+    heads = range(2)
+
+    def scale(v):
+        v = v.astype(F32)
+        return lax.rsqrt(jnp.sum(v * v, axis=1, keepdims=True) + 1.0)
+
+    def head_of(s, i, h):
+        return pj[s, i, :, h * E : (h + 1) * E]
+
+    def chain_terms(s, bd):
         lane = lax.broadcasted_iota(jnp.int32, (L, PAD), 1)
         bias = jnp.where(lane == 0, bias_ref[0], jnp.where(lane == 1, bias_ref[1], 0.0))
         rate = jnp.where(lane == 2, rate_ref[0], jnp.where(lane == 3, rate_ref[1], 0.0))
@@ -248,16 +280,8 @@
         g = -jnp.exp(rate) * soft
         tri = jnp.where(lower, 1.0, 0.0).astype(BF)
         cum = sum(dot(tri, part) for part in split3(g))
-        heads = range(2)
-        qs = [pj[s, 0, :, h * E : (h + 1) * E] for h in heads]
-        ks = [pj[s, 1, :, h * E : (h + 1) * E] for h in heads]
-        vs = [pj[s, 2, :, h * E : (h + 1) * E] for h in heads]
-
-        def scale(v):
-            v = v.astype(F32)
-            return lax.rsqrt(jnp.sum(v * v, axis=1, keepdims=True) + 1.0)
-
-        rq = [scale(v) for v in qs]
+        ks = [head_of(s, 1, h) for h in heads]
+        vs = [head_of(s, 2, h) for h in heads]
         rk = [scale(v) for v in ks]
         pack = jnp.where(lane == 0, rk[0], jnp.where(lane == 1, rk[1], cum))
         eye = jnp.where(
@@ -267,7 +291,7 @@
             0.0,
         ).astype(BF)
         rows = sum(dot_nt(eye, part) for part in split3(pack))
-        amats, scores, cumc, betac = [], [], [], []
+        amats, cumc, betac = [], [], []
         for h in heads:
             cc = cum[:, 2 + h : 3 + h]
             bc = beta[:, h : h + 1]
@@ -277,9 +301,7 @@
             crow = rows[2 + h : 3 + h, :]
             decay = jnp.exp(jnp.where(lower, cc - crow, 0.0)) * rrow
             kk = dot_nt(ks[h], ks[h])
-            qk = dot_nt(qs[h], ks[h])
             amats.append(jnp.where(strict, kk * (bc * rk[h]) * decay, 0.0))
-            scores.append(jnp.where(lower, qk * rq[h] * decay, 0.0).astype(BF))
 
         def level_mask(bit):
             return ((it >> (bit + 1)) == (js >> (bit + 1))) & ((it >> bit) != (js >> bit))
@@ -306,11 +328,22 @@
             last = cumc[h][L - 1 : L, :]
             kd = kf * (rk[h] * jnp.exp(last - cumc[h]))
             rs = dot_tn(kd.astype(BF), sb)
-            sx = dot(scores[h], sb)
             a = jnp.broadcast_to(jnp.exp(last), (1, E))
             write_map(msg.at[b], a, rs[:, :E], rs[:, E:])
+            sols[b] = sb
+        return cumc, rows
+
+    def out_terms(s, cumc, rows):
+        for h in heads:
+            b = 2 * s + h
+            q, k = head_of(s, 0, h), head_of(s, 1, h)
+            rq = scale(q)
+            cc = cumc[h]
+            decay = jnp.exp(jnp.where(lower, cc - rows[2 + h : 3 + h, :], 0.0)) * rows[h : h + 1, :]
+            score = jnp.where(lower, dot_nt(q, k) * rq * decay, 0.0).astype(BF)
+            sx = dot(score, sols[b])
             lo[b] = sx[:, E:]
-            qd = qs[h].astype(F32) * (rq[h] * ecum)
+            qd = q.astype(F32) * (rq * jnp.exp(cc))
             reach[b] = (qd - sx[:, :E]).astype(BF)
 
     def xcopy(b, src_x):
@@ -338,19 +371,25 @@
     send_own(0)
     forward(0)
     send_own(1)
-    finish_gather(0)
+    finish_near(0)
+    finish_far(0)
     for cp in wcopies:
         cp.wait()
-    project(0)
+    project(0, (1, 2))
     forward(1)
-    local_terms(0)
+    kept0 = chain_terms(0, small(0))
     xsend(0)
     xsend(1)
-    finish_gather(1)
-    project(1)
-    local_terms(1)
+    project(0, (0, 3))
+    out_terms(0, *kept0)
+    finish_near(1)
+    part = near(1)
+    finish_far(1)
+    kept1 = chain_terms(1, far(1, part))
     xsend(2)
     xsend(3)
+    project(1, (0, 3))
+    out_terms(1, *kept1)
 
     for j in range(NX):
 
@@ -384,26 +423,36 @@
             device_id_type=MESH,
         )
 
-    for step in range(1, 5):
+    def zmap(k, valid):
+        a, r, v = read_map(zin.at[lax.rem(k + NZ, NZ)])
+        return (
+            jnp.where(valid, a, 1.0),
+            jnp.where(valid, r, 0.0),
+            jnp.where(valid, v, 0.0),
+        )
+
+    behind = None
+    early = None
+    for step in range(1, 6):
         for piece in range(2):
             for direction in range(2):
-                if direction == 1 and step > 3:
-                    continue
                 slot = zslot(step, direction)
-                if step > 1:
+                if step > 1 and step - 1 <= 4 - direction:
                     zcopy(step - 1, piece, direction, slot).wait_recv()
-                zcopy(step, piece, direction, slot).start()
-    m210 = compose(maps[2], m10)
-    for piece in range(2):
-        zcopy(3, piece, 1, zslot(4, 1)).wait_recv()
-        zcopy(4, piece, 0, zslot(5, 0)).wait_recv()
-
-    state = jnp.zeros((E, E), F32)
-    here = state
-    for k in range(NZ):
-        here = jnp.where(z == k, state, here)
-        m = read_map(zin.at[k])
-        state = m[2] if k == 0 else apply_map(m, state)
+                if step <= 4 - direction:
+                    zcopy(step, piece, direction, slot).start()
+        if step == 1:
+            m210 = compose(maps[2], m10)
+            continue
+        dist = step - 1
+        if dist <= 3:
+            found = zmap(z + dist, z + dist >= NZ)
+            early = found[2] if early is None else apply_map(found, early)
+            found = zmap(z - dist, z - dist >= 0)
+            behind = found if behind is None else compose(behind, found)
+        else:
+            early = apply_map(zmap(z - dist, z - dist >= 0), early)
+    here = apply_map(behind, early)
     starts = [here] + [apply_map(m, here) for m in (maps[0], m10, m210)]
 
     def rcopy(j, b):
@@ -442,6 +491,10 @@
         @pl.when(x == j)
         def _():
             rlocal(j).start()
+
+    state = read_map(zin.at[0])[2]
+    for k in range(1, NZ):
+        state = apply_map(read_map(zin.at[k]), state)
 
     memory = state.astype(BF)
 
@@ -544,6 +597,12 @@
                 if direction == 1 and step > 3:
                     continue
                 zcopy(step, piece, direction, zslot(step, direction)).wait_send()
+
+
+def hand_over(mixed_in, cache_in, first_in, mixed_out, cache_out, first_out):
+    mixed_out[...] = mixed_in[...]
+    cache_out[...] = cache_in[...]
+    first_out[...] = first_in[...]
 
 
 def shards(
@@ -563,9 +622,6 @@
     new_beta,
     new_decay,
 ):
-    wbd = jnp.concatenate(
-        [beta_weight.T, decay_weight.T, jnp.zeros((PAD - 4, D), BF)], axis=0
-    )
     smem = pl.BlockSpec(memory_space=pltpu.SMEM)
     vmem = pl.BlockSpec(memory_space=pltpu.VMEM)
     hbm = pl.BlockSpec(memory_space=pl.ANY)
@@ -577,14 +633,17 @@
             jax.ShapeDtypeStruct((2, 2, 4, E), BF),
             jax.ShapeDtypeStruct((2, 2 * E), F32),
         ),
-        in_specs=[smem] * 4 + [hbm] * 5 + [vmem] * 5,
+        in_specs=[smem] * 4 + [hbm] * 5 + [vmem] * 6,
         out_specs=(vmem, vmem, vmem),
         scratch_shapes=[
             pltpu.VMEM((2, L, D), BF),
             pltpu.VMEM((4, D, 2 * E), BF),
             pltpu.VMEM((2, 4, L, 2 * E), BF),
+            pltpu.VMEM((2, L, 2 * E), F32),
+            pltpu.VMEM((PAD, D), BF),
             pltpu.VMEM((4, L, E), F32),
             pltpu.VMEM((4, L, E), BF),
+            pltpu.VMEM((4, L, 2 * E), BF),
             pltpu.VMEM((4, 2, E + PAD, E), BF),
             pltpu.VMEM((4, 2, E + PAD, E), BF),
             pltpu.VMEM((NZ, 2, E + PAD, E), BF),
@@ -623,13 +682,20 @@
         key_weight,
         value_weight,
         gate_weight,
-        wbd,
+        beta_weight.T,
+        decay_weight.T,
         out_gain.reshape(1, E),
         new_query,
         new_key,
         new_value,
     )
-    return out
+    return pl.pallas_call(
+        hand_over,
+        out_shape=tuple(jax.ShapeDtypeStruct(o.shape, o.dtype) for o in out),
+        in_specs=[vmem] * 3,
+        out_specs=(vmem,) * 3,
+        name="hand_over",
+    )(*out)
 
 
 def solution(mesh):

time: 67.9 us -> 64 us (0.943)
  local copies, waits for them, and re-layouts: 4.19 us -> 0 us
  Pallas kernels: 61.2 us -> 63.2 us
  other arithmetic: 1.47 us -> 0 us
    unnamed x3 -> x0, local copies, waits for them, and re-layouts: 4.11 us -> none
    pallas_call x0 -> x1, Pallas kernels: none -> 1.63 us  [shards(): pl.pallas_call(hand_over, out_shape=tuple((jax.ShapeDtypeStruct(o.shape,...]
    concatenate x1 -> x0, other arithmetic: 1.47 us -> none  [shards(): jnp.concatenate([beta_weight.T, decay_weight.T, jnp.zeros((PAD - 4, D), B...]
where the time goes in v2:
time: 64 us; the launch traced here: 63.9 us
  Pallas kernels  63.2 us (99%)
  between operations  0.65 us (1%)
    pallas_call x1, Pallas kernels, shards(): pl.pallas_call(kernel, out_shape=(jax.ShapeDtypeStruct((2, L, 2 * E), BF)...  61.6 us
    pallas_call x1, Pallas kernels, shards(): pl.pallas_call(hand_over, out_shape=tuple((jax.ShapeDtypeStruct(o.shape,...  1.63 us

profile of v2, /device:TPU:32, one launch (start us, length us, event | category | flops | bytes accessed | tf_op | source)
XLA Modules:
  0.0 63.9 jit_solution(2940913007723750648)
XLA Ops:
  0.6 61.6 %delta_all.1 = (bf16[2,192,256]{2,1,0:T(8,128)(2,1)}, bf16[2,2,4,128]{3,2,1,0:T(4,128)(2,1)}, f32[2,256]{1,0:T(2,128)}) custom-call(f32[2]{0:T(128)} %bias_ref.1, f32[2]{0:T(128)} %rate_ref.1, f32[2,2]{1,0:T(2,128)} %nbeta_ref.1, f32[2,2]{1,0:T(2,128)} %ndecay_ref.1, bf16[2,192,512]{2,1,0:T(8,128)(2,1)} %tok_ref.1, bf16[4096,256]{1,0:T(8,128)(2,1)} %wq_ref.1, ...), custom_call_target="tpu_custom_call" | custom-call | tf_op jit(solution)/shard_map/delta_all/pallas_call | solution.py:629
  62.3 1.6 %hand_over.1 = (bf16[2,192,256]{2,1,0:T(8,128)(2,1)}, bf16[2,2,4,128]{3,2,1,0:T(4,128)(2,1)}, f32[2,256]{1,0:T(2,128)}) custom-call(bf16[2,192,256]{2,1,0:T(8,128)(2,1)} %get-tuple-element.6.mixed_in, bf16[2,2,4,128]{3,2,1,0:T(4,128)(2,1)} %get-tuple-element.7.cache_in, f32[2,256]{1,0:T(2,128)} %get-tuple-element.8.first_in), custom_call_target="tpu_custom_call" | custom-call | tf_op jit(solution)/shard_map/hand_over/pallas_call | solution.py:692

commit v3 on v2

--- a/solution.py
+++ b/solution.py
@@ -16,6 +16,9 @@
 KC = 512
 D = 4096
 PAD = 16
+HE = E // 2
+ROWS = E + HE + PAD
+PIECES = ((0, 112), (112, 96))
 
 
 def dot(a, b):
@@ -39,36 +42,29 @@
 
 
 def compose(later, earlier):
-    al, rl, sl = later
-    ae, re, se = earlier
-    prod = dot(rl.astype(BF), jnp.concatenate([re, se], axis=1).astype(BF))
-    r = al * re + ae * rl - prod[:, :E]
-    s = al * se + sl - prod[:, E:]
-    return al * ae, r, s
+    al, xl = later
+    ae, xe = earlier
+    grown = jnp.concatenate([ae * xl[:E], xl[E:]], axis=0)
+    return al * ae, al * xe + grown - dot(xe.astype(BF), xl[:E].astype(BF))
 
 
 def apply_map(m, state):
-    a, r, s = m
-    return a * state - dot(r.astype(BF), state.astype(BF)) + s
-
-
-def write_map(ref, a, r, s):
-    ref[0, 0:E, :] = r.astype(BF)
+    a, x = m
+    return a * state - dot(state.astype(BF), x[:E].astype(BF)) + x[E:]
+
+
+def tail_rows(a):
     hi, mid, low = split3(a)
     row = lax.broadcasted_iota(jnp.int32, (PAD, E), 0)
-    tail = jnp.where(
+    return jnp.where(
         row == 0,
         hi.astype(F32),
         jnp.where(row == 1, mid.astype(F32), jnp.where(row == 2, low.astype(F32), 0.0)),
-    )
-    ref[0, E : E + PAD, :] = tail.astype(BF)
-    ref[1, 0:E, :] = s.astype(BF)
-
-
-def read_map(ref):
-    tail = ref[0, E : E + PAD, :].astype(F32)
-    a = jnp.sum(tail, axis=0, keepdims=True)
-    return a, ref[0, 0:E, :].astype(F32), ref[1, 0:E, :].astype(F32)
+    ).astype(BF)
+
+
+def tail_value(rows):
+    return jnp.sum(rows.astype(F32), axis=0, keepdims=True)
 
 
 def kernel(
@@ -125,8 +121,11 @@
     z, x, y, c = (lax.axis_index(n) for n in ("z", "x", "y", "c"))
     yu, yd = lax.rem(y + 1, NY), lax.rem(y + NY - 1, NY)
     yf = lax.rem(y + 2, NY)
-    zu, zd = lax.rem(z + 1, NZ), lax.rem(z + NZ - 1, NZ)
+    head, side_half = x // 2, lax.rem(x, 2)
     other = 1 - c
+
+    def z_at(d):
+        return lax.rem(z + d + NZ, NZ)
 
     def cols(yy, cc):
         return pl.ds(pl.multiple_of((yy * NC + cc) * KC, KC), KC)
@@ -148,7 +147,8 @@
     ).astype(BF)
 
     barrier = pltpu.get_barrier_semaphore()
-    partners = [{"y": yu}, {"y": yd}, {"c": other}, {"z": zu}, {"z": zd}]
+    partners = [{"y": yu}, {"y": yd}, {"c": other}]
+    partners += [{"z": z_at(d)} for d in (1, -1, 2, -2)]
     partners += [{"x": lax.rem(x + d, NX)} for d in (1, 2, 3)]
     for p in partners:
         pl.semaphore_signal(barrier, inc=1, device_id=p, device_id_type=MESH)
@@ -327,9 +327,11 @@
             sb = sol.astype(BF)
             last = cumc[h][L - 1 : L, :]
             kd = kf * (rk[h] * jnp.exp(last - cumc[h]))
-            rs = dot_tn(kd.astype(BF), sb)
-            a = jnp.broadcast_to(jnp.exp(last), (1, E))
-            write_map(msg.at[b], a, rs[:, :E], rs[:, E:])
+            rs = dot_tn(sb, kd.astype(BF)).astype(BF)
+            msg[s, h, 0:HE, :] = rs[E : E + HE]
+            msg[s, h, HE : HE + E, :] = rs[:E]
+            msg[s, h, HE + E : ROWS, :] = tail_rows(jnp.broadcast_to(jnp.exp(last), (1, E)))
+            msg[s, h, ROWS:, :] = rs[E + HE :]
             sols[b] = sb
         return cumc, rows
 
@@ -346,27 +348,200 @@
             qd = q.astype(F32) * (rq * jnp.exp(cc))
             reach[b] = (qd - sx[:, :E]).astype(BF)
 
-    def xcopy(b, src_x):
-        return pltpu.make_async_remote_copy(
-            src_ref=msg.at[b],
-            dst_ref=xin.at[src_x],
-            send_sem=xs_sem.at[b],
-            recv_sem=xr_sem.at[src_x],
-            device_id={"x": b},
-            device_id_type=MESH,
-        )
-
-    def xlocal(b):
-        return pltpu.make_async_copy(msg.at[b], xin.at[b], xs_sem.at[b])
-
-    def xsend(b):
-        @pl.when(x != b)
-        def _():
-            xcopy(b, x).start()
-
-        @pl.when(x == b)
-        def _():
-            xlocal(b).start()
+    def xpart(s, t):
+        return msg.at[s, t // 2, pl.ds(HE * (t % 2), ROWS)]
+
+    def xcopy(s, t, src_x):
+        return pltpu.make_async_remote_copy(
+            src_ref=xpart(s, t),
+            dst_ref=xin.at[s, src_x],
+            send_sem=xs_sem.at[s, t],
+            recv_sem=xr_sem.at[s, src_x],
+            device_id={"x": t},
+            device_id_type=MESH,
+        )
+
+    def xlocal(s, t):
+        return pltpu.make_async_copy(xpart(s, t), xin.at[s, t], xs_sem.at[s, t])
+
+    def spread(remote, local):
+        for t in range(NX):
+
+            @pl.when(x != t)
+            def _():
+                remote(t).start()
+
+            @pl.when(x == t)
+            def _():
+                local(t).start()
+
+    def collect(remote, local):
+        for t in range(NX):
+
+            @pl.when(x != t)
+            def _():
+                remote(t).wait_recv()
+
+            @pl.when(x == t)
+            def _():
+                local(t).wait()
+
+    def xsend(s):
+        spread(lambda t: xcopy(s, t, x), lambda t: xlocal(s, t))
+
+    def zcopy(s, slot, piece, hop, dist):
+        first, count = PIECES[piece]
+        part = zin.at[s, slot, pl.ds(first, count)]
+        return pltpu.make_async_remote_copy(
+            src_ref=part,
+            dst_ref=part,
+            send_sem=zs_sem.at[s, dist % NZ, piece],
+            recv_sem=zr_sem.at[s, dist % NZ, piece],
+            device_id={"z": z_at(hop)},
+            device_id_type=MESH,
+        )
+
+    def zsend(s):
+        collect(lambda t: xcopy(s, t, t), lambda t: xlocal(s, t))
+        maps = []
+        for j in range(NX):
+            r = xin[s, j, pl.ds(pl.multiple_of(HE * (1 - side_half), PAD), E), :]
+            a = xin[s, j, pl.ds(pl.multiple_of(E + HE - HE * side_half, PAD), PAD), :]
+            v = xin[s, j, pl.ds(pl.multiple_of((E + PAD) * side_half, PAD), HE), :]
+            maps.append((tail_value(a), jnp.concatenate([r, v], axis=0).astype(F32)))
+        m10 = compose(maps[1], maps[0])
+        m32 = compose(maps[3], maps[2])
+        a, total = compose(m32, m10)
+        zin[s, z, 0 : E + HE, :] = total.astype(BF)
+        zin[s, z, E + HE : ROWS, :] = tail_rows(a)
+        for hop in (2, -2, 1, -1):
+            for piece in range(2):
+                zcopy(s, z, piece, hop, hop).start()
+        return maps[0], m10, maps[2]
+
+    def zrelay(s):
+        for piece in range(2):
+            for d in (1, -1):
+                slot = z_at(-2 * d)
+                zcopy(s, slot, piece, 1, 2 * d).wait_recv()
+                zcopy(s, slot, piece, d, 3 * d).start()
+                if (piece == 0) == (d == 1):
+                    zcopy(s, slot, piece, 2 * d, 4).start()
+
+    def zwait(s, *dists):
+        for d in dists:
+            for piece in range(2):
+                zcopy(s, z_at(-d), piece, 1, d).wait_recv()
+
+    def zmap(s, slot):
+        return tail_value(zin[s, slot, E + HE : ROWS, :]), zin[s, slot, 0 : E + HE, :].astype(F32)
+
+    def zmap_if(s, d):
+        valid = z + d >= NZ if d > 0 else z + d >= 0
+        a, m = zmap(s, z_at(d))
+        return jnp.where(valid, a, 1.0), jnp.where(valid, m, 0.0)
+
+    def rcopy(s, t, src_x):
+        return pltpu.make_async_remote_copy(
+            src_ref=ret.at[s, t],
+            dst_ref=pin.at[s, src_x],
+            send_sem=rs_sem.at[s, t],
+            recv_sem=rr_sem.at[s, src_x],
+            device_id={"x": t},
+            device_id_type=MESH,
+        )
+
+    def rlocal(s, t):
+        return pltpu.make_async_copy(ret.at[s, t], pin.at[s, t], rs_sem.at[s, t])
+
+    def scopy(s, t, src_x):
+        return pltpu.make_async_remote_copy(
+            src_ref=side.at[s, t],
+            dst_ref=sin.at[s, src_x],
+            send_sem=ss_sem.at[s, t],
+            recv_sem=sr_sem.at[s, src_x],
+            device_id={"x": t},
+            device_id_type=MESH,
+        )
+
+    def slocal(s, t):
+        return pltpu.make_async_copy(side.at[s, t], sin.at[s, t], ss_sem.at[s, t])
+
+    def start_states(s, inner):
+        zwait(s, 1, -1)
+        behind = compose(zmap_if(s, -1), zmap_if(s, -2))
+        early = apply_map(zmap_if(s, 2), zmap_if(s, 1)[1][E:])
+        zwait(s, 3, -3, 4)
+        behind = compose(behind, zmap_if(s, -3))
+        early = apply_map(zmap_if(s, -4), apply_map(zmap_if(s, 3), early))
+        here = apply_map(behind, early)
+        m0, m10, m2 = inner
+        second = apply_map(m10, here)
+        ret[s, 0] = here.astype(BF)
+        ret[s, 1] = apply_map(m0, here).astype(BF)
+        ret[s, 2] = second.astype(BF)
+        ret[s, 3] = apply_map(m2, second).astype(BF)
+        spread(lambda t: rcopy(s, t, x), lambda t: rlocal(s, t))
+
+    def unit(v):
+        return v * lax.rsqrt(jnp.sum(v * v, axis=1, keepdims=True) + 1.0)
+
+    gain = gain_ref[...]
+
+    def final_parts(s):
+        state = apply_map(zmap(s, 1), zmap(s, 0)[1][E:])
+        for k in (2, 4, 6):
+            state = apply_map(compose(zmap(s, k + 1), zmap(s, k)), state)
+        place = lax.broadcasted_iota(jnp.int32, (HE, E), 1) == (
+            lax.broadcasted_iota(jnp.int32, (HE, E), 0) + HE * side_half
+        )
+        memf = dot_tn(state.astype(BF), jnp.where(place, 1.0, 0.0).astype(BF))
+        memory = memf.astype(BF)
+
+        def pick(ref):
+            row = ref[s].astype(F32)
+            return jnp.where(head == 0, row[0:1, :], row[1:2, :])
+
+        qn, kn, nv = unit(pick(nq_ref)), unit(pick(nk_ref)), pick(nv_ref)
+        nbeta = jnp.where(head == 0, nbeta_ref[s, 0], nbeta_ref[s, 1])
+        ndecay = jnp.where(head == 0, ndecay_ref[s, 0], ndecay_ref[s, 1])
+        row = lax.broadcasted_iota(jnp.int32, (PAD, E), 0)
+        asked = jnp.where(row == 0, qn, jnp.where(row == 1, kn, 0.0))
+        seen = sum(dot(part, memory) for part in split3(asked))
+        recall, retrieve = seen[0:1, :], seen[1:2, :]
+        intersect = jnp.sum(kn * qn, axis=1, keepdims=True)
+        lane = lax.broadcasted_iota(jnp.int32, (1, E), 1)
+        nv = jnp.where((lane >= HE) == (side_half == 1), nv, 0.0)
+        fresh = nv - ndecay * retrieve
+        read = ndecay * recall + (nbeta * intersect) * fresh
+        mine = memf[0:16, :]
+        for k in range(1, NZ):
+            mine = jnp.where(z == k, memf[16 * k : 16 * k + 16, :], mine)
+        for t in range(NX):
+            side[s, t, 0:4, :] = mine[4 * t : 4 * t + 4, :]
+            side[s, t, 4:8, :] = jnp.broadcast_to(read, (4, E))
+        spread(lambda t: scopy(s, t, x), lambda t: slocal(s, t))
+
+    def outputs(s):
+        collect(lambda t: rcopy(s, t, t), lambda t: rlocal(s, t))
+        for h in heads:
+            b = 2 * s + h
+            start = jnp.concatenate([pin[s, 2 * h], pin[s, 2 * h + 1]], axis=0)
+            o = lo[b] + dot_nt(reach[b], start)
+            gate = head_of(s, 3, h).astype(F32)
+            norm = lax.rsqrt(jnp.mean(o * o, axis=1, keepdims=True) + 0.001)
+            out_ref[s, :, h * E : (h + 1) * E] = (
+                o * norm * gain * (gate * jax.nn.sigmoid(gate))
+            ).astype(BF)
+
+    def last_parts(s):
+        collect(lambda t: scopy(s, t, t), lambda t: slocal(s, t))
+        for h in heads:
+            both = sin[s, 2 * h] + sin[s, 2 * h + 1]
+            cache_ref[s, h] = both[0:4].astype(BF)
+            read = both[4:5]
+            norm = lax.rsqrt(jnp.mean(read * read, axis=1, keepdims=True) + 0.001)
+            first_ref[s : s + 1, h * E : (h + 1) * E] = read * norm * gain
 
     send_own(0)
     forward(0)
@@ -379,201 +554,27 @@
     forward(1)
     kept0 = chain_terms(0, small(0))
     xsend(0)
-    xsend(1)
     project(0, (0, 3))
     out_terms(0, *kept0)
     finish_near(1)
     part = near(1)
+    inner0 = zsend(0)
     finish_far(1)
     kept1 = chain_terms(1, far(1, part))
-    xsend(2)
-    xsend(3)
+    xsend(1)
+    zrelay(0)
     project(1, (0, 3))
     out_terms(1, *kept1)
-
-    for j in range(NX):
-
-        @pl.when(x != j)
-        def _():
-            xcopy(j, j).wait_recv()
-
-        @pl.when(x == j)
-        def _():
-            xlocal(j).wait()
-
-    maps = [read_map(xin.at[j]) for j in range(NX)]
-    m10 = compose(maps[1], maps[0])
-    m32 = compose(maps[3], maps[2])
-    total = compose(m32, m10)
-    write_map(zin.at[z], *total)
-
-    def zslot(step, direction):
-        if direction == 0:
-            return lax.rem(z + NZ - (step - 1), NZ)
-        return lax.rem(z + (step - 1), NZ)
-
-    def zcopy(step, piece, direction, slot):
-        part = zin.at[slot, piece]
-        return pltpu.make_async_remote_copy(
-            src_ref=part,
-            dst_ref=part,
-            send_sem=zs_sem.at[step - 1, piece, direction],
-            recv_sem=zr_sem.at[step - 1, piece, direction],
-            device_id={"z": zu if direction == 0 else zd},
-            device_id_type=MESH,
-        )
-
-    def zmap(k, valid):
-        a, r, v = read_map(zin.at[lax.rem(k + NZ, NZ)])
-        return (
-            jnp.where(valid, a, 1.0),
-            jnp.where(valid, r, 0.0),
-            jnp.where(valid, v, 0.0),
-        )
-
-    behind = None
-    early = None
-    for step in range(1, 6):
-        for piece in range(2):
-            for direction in range(2):
-                slot = zslot(step, direction)
-                if step > 1 and step - 1 <= 4 - direction:
-                    zcopy(step - 1, piece, direction, slot).wait_recv()
-                if step <= 4 - direction:
-                    zcopy(step, piece, direction, slot).start()
-        if step == 1:
-            m210 = compose(maps[2], m10)
-            continue
-        dist = step - 1
-        if dist <= 3:
-            found = zmap(z + dist, z + dist >= NZ)
-            early = found[2] if early is None else apply_map(found, early)
-            found = zmap(z - dist, z - dist >= 0)
-            behind = found if behind is None else compose(behind, found)
-        else:
-            early = apply_map(zmap(z - dist, z - dist >= 0), early)
-    here = apply_map(behind, early)
-    starts = [here] + [apply_map(m, here) for m in (maps[0], m10, m210)]
-
-    def rcopy(j, b):
-        return pltpu.make_async_remote_copy(
-            src_ref=ret.at[j],
-            dst_ref=pin.at[b],
-            send_sem=rs_sem.at[j],
-            recv_sem=rr_sem.at[b],
-            device_id={"x": j},
-            device_id_type=MESH,
-        )
-
-    def rlocal(j):
-        return pltpu.make_async_copy(ret.at[j], pin.at[j], rs_sem.at[j])
-
-    def scopy(j, b):
-        return pltpu.make_async_remote_copy(
-            src_ref=side.at[j],
-            dst_ref=sin.at[b],
-            send_sem=ss_sem.at[j],
-            recv_sem=sr_sem.at[b],
-            device_id={"x": j},
-            device_id_type=MESH,
-        )
-
-    def slocal(j):
-        return pltpu.make_async_copy(side.at[j], sin.at[j], ss_sem.at[j])
-
-    for j in range(NX):
-        ret[j] = starts[j].astype(BF)
-
-        @pl.when(x != j)
-        def _():
-            rcopy(j, x).start()
-
-        @pl.when(x == j)
-        def _():
-            rlocal(j).start()
-
-    state = read_map(zin.at[0])[2]
-    for k in range(1, NZ):
-        state = apply_map(read_map(zin.at[k]), state)
-
-    memory = state.astype(BF)
-
-    def pick(ref):
-        row = ref[0, 0:1, :].astype(F32)
-        for b in range(1, 4):
-            row = jnp.where(x == b, ref[b // 2, b % 2 : b % 2 + 1, :].astype(F32), row)
-        return row
-
-    def pick_scalar(ref):
-        value = ref[0, 0]
-        for b in range(1, 4):
-            value = jnp.where(x == b, ref[b // 2, b % 2], value)
-        return value
-
-    def unit(v):
-        return v * lax.rsqrt(jnp.sum(v * v, axis=1, keepdims=True) + 1.0)
-
-    qn, kn, nv = unit(pick(nq_ref)), unit(pick(nk_ref)), pick(nv_ref)
-    nbeta, ndecay = pick_scalar(nbeta_ref), pick_scalar(ndecay_ref)
-    row8 = lax.broadcasted_iota(jnp.int32, (PAD, E), 0)
-    probe = jnp.where(row8 == 0, qn, jnp.where(row8 == 1, kn, 0.0))
-    seen = sum(dot(part, memory) for part in split3(probe))
-    recall, retrieve = seen[0:1, :], seen[1:2, :]
-    intersect = jnp.sum(kn * qn, axis=1, keepdims=True)
-    fresh = nv - ndecay * retrieve
-    read = ndecay * recall + (nbeta * intersect) * fresh
-    gain = gain_ref[...]
-    first = read * lax.rsqrt(jnp.mean(read * read, axis=1, keepdims=True) + 0.001) * gain
-
-    memf = memory.astype(F32)
-    mine = memf[0:16, :]
-    for k in range(1, NZ):
-        mine = jnp.where(z == k, memf[16 * k : 16 * k + 16, :], mine)
-    for j in range(NX):
-        side[j, 0:4, :] = mine[4 * j : 4 * j + 4, :]
-        side[j, 4:8, :] = jnp.broadcast_to(first, (4, E))
-
-        @pl.when(x != j)
-        def _():
-            scopy(j, x).start()
-
-        @pl.when(x == j)
-        def _():
-            slocal(j).start()
-
-    for b in range(4):
-
-        @pl.when(x != b)
-        def _():
-            rcopy(b, b).wait_recv()
-
-        @pl.when(x == b)
-        def _():
-            rlocal(b).wait()
-
-    for b in range(4):
-        s, h = b // 2, b % 2
-        o = lo[b] + dot(reach[b], pin[b])
-        gate = pj[s, 3, :, h * E : (h + 1) * E].astype(F32)
-        norm = lax.rsqrt(jnp.mean(o * o, axis=1, keepdims=True) + 0.001)
-        out_ref[s, :, h * E : (h + 1) * E] = (
-            o * norm * gain * (gate * jax.nn.sigmoid(gate))
-        ).astype(BF)
-
-    for b in range(4):
-
-        @pl.when(x != b)
-        def _():
-            scopy(b, b).wait_recv()
-
-        @pl.when(x == b)
-        def _():
-            slocal(b).wait()
-
-    for b in range(4):
-        s, h = b // 2, b % 2
-        cache_ref[s, h] = sin[b, 0:4, :].astype(BF)
-        first_ref[s : s + 1, h * E : (h + 1) * E] = sin[b, 4:5, :]
+    inner1 = zsend(1)
+    start_states(0, inner0)
+    zrelay(1)
+    final_parts(0)
+    outputs(0)
+    start_states(1, inner1)
+    final_parts(1)
+    last_parts(0)
+    outputs(1)
+    last_parts(1)
 
     for s in range(2):
         for half in range(2):
@@ -583,20 +584,22 @@
             fcopy(s, direction).wait_send()
         for k in range(4):
             pcopy(s, k, c).wait_send()
-    for j in range(NX):
-
-        @pl.when(x != j)
-        def _():
-            xcopy(j, x).wait_send()
-            rcopy(j, x).wait_send()
-            scopy(j, x).wait_send()
-
-    for step in range(1, 5):
+        for t in range(NX):
+
+            @pl.when(x != t)
+            def _():
+                xcopy(s, t, x).wait_send()
+                rcopy(s, t, x).wait_send()
+                scopy(s, t, x).wait_send()
+
+        for hop in (2, -2, 1, -1):
+            for piece in range(2):
+                zcopy(s, z, piece, hop, hop).wait_send()
         for piece in range(2):
-            for direction in range(2):
-                if direction == 1 and step > 3:
-                    continue
-                zcopy(step, piece, direction, zslot(step, direction)).wait_send()
+            for d in (1, -1):
+                zcopy(s, z_at(-2 * d), piece, d, 3 * d).wait_send()
+                if (piece == 0) == (d == 1):
+                    zcopy(s, z_at(-2 * d), piece, 2 * d, 4).wait_send()
 
 
 def hand_over(mixed_in, cache_in, first_in, mixed_out, cache_out, first_out):
@@ -644,13 +647,13 @@
             pltpu.VMEM((4, L, E), F32),
             pltpu.VMEM((4, L, E), BF),
             pltpu.VMEM((4, L, 2 * E), BF),
-            pltpu.VMEM((4, 2, E + PAD, E), BF),
-            pltpu.VMEM((4, 2, E + PAD, E), BF),
-            pltpu.VMEM((NZ, 2, E + PAD, E), BF),
-            pltpu.VMEM((4, E, E), BF),
-            pltpu.VMEM((4, E, E), BF),
-            pltpu.VMEM((4, 8, E), F32),
-            pltpu.VMEM((4, 8, E), F32),
+            pltpu.VMEM((2, 2, E + 2 * HE + PAD, E), BF),
+            pltpu.VMEM((2, NX, ROWS, E), BF),
+            pltpu.VMEM((2, NZ, ROWS, E), BF),
+            pltpu.VMEM((2, NX, HE, E), BF),
+            pltpu.VMEM((2, NX, HE, E), BF),
+            pltpu.VMEM((2, NX, 8, E), F32),
+            pltpu.VMEM((2, NX, 8, E), F32),
             dma((4,)),
             dma((2,)),
             dma((2, 2, 2)),
@@ -659,14 +662,14 @@
             dma((2, 2)),
             dma((2, 4)),
             dma((2, 4)),
-            dma((4,)),
-            dma((4,)),
-            dma((4, 2, 2)),
-            dma((4, 2, 2)),
-            dma((4,)),
-            dma((4,)),
-            dma((4,)),
-            dma((4,)),
+            dma((2, NX)),
+            dma((2, NX)),
+            dma((2, NZ, 2)),
+            dma((2, NZ, 2)),
+            dma((2, NX)),
+            dma((2, NX)),
+            dma((2, NX)),
+            dma((2, NX)),
         ],
         compiler_params=pltpu.CompilerParams(
             collective_id=0, has_side_effects=True, vmem_limit_bytes=60 * 1024 * 1024

time: 64 us -> 61.2 us (0.956)
  Pallas kernels: 63.2 us -> 60.4 us
    pallas_call x1, Pallas kernels: 61.6 us -> 58.8 us  [shards(): pl.pallas_call(kernel, out_shape=(jax.ShapeDtypeStruct((2, L, 2 * E), BF)...]
where the time goes in v3:
time: 61.2 us; the launch traced here: 61.1 us
  Pallas kernels  60.4 us (99%)
  between operations  0.65 us (1%)
    pallas_call x1, Pallas kernels, shards(): pl.pallas_call(kernel, out_shape=(jax.ShapeDtypeStruct((2, L, 2 * E), BF)...  58.8 us
    pallas_call x1, Pallas kernels, shards(): pl.pallas_call(hand_over, out_shape=tuple((jax.ShapeDtypeStruct(o.shape,...  1.63 us

profile of v3, /device:TPU:32, one launch (start us, length us, event | category | flops | bytes accessed | tf_op | source)
XLA Modules:
  0.0 61.1 jit_solution(9880323095433267357)
XLA Ops:
  0.6 58.8 %delta_all.1 = (bf16[2,192,256]{2,1,0:T(8,128)(2,1)}, bf16[2,2,4,128]{3,2,1,0:T(4,128)(2,1)}, f32[2,256]{1,0:T(2,128)}) custom-call(f32[2]{0:T(128)} %bias_ref.1, f32[2]{0:T(128)} %rate_ref.1, f32[2,2]{1,0:T(2,128)} %nbeta_ref.1, f32[2,2]{1,0:T(2,128)} %ndecay_ref.1, bf16[2,192,512]{2,1,0:T(8,128)(2,1)} %tok_ref.1, bf16[4096,256]{1,0:T(8,128)(2,1)} %wq_ref.1, ...), custom_call_target="tpu_custom_call" | custom-call | tf_op jit(solution)/shard_map/delta_all/pallas_call | solution.py:632
  59.4 1.6 %hand_over.1 = (bf16[2,192,256]{2,1,0:T(8,128)(2,1)}, bf16[2,2,4,128]{3,2,1,0:T(4,128)(2,1)}, f32[2,256]{1,0:T(2,128)}) custom-call(bf16[2,192,256]{2,1,0:T(8,128)(2,1)} %get-tuple-element.6.mixed_in, bf16[2,2,4,128]{3,2,1,0:T(4,128)(2,1)} %get-tuple-element.7.cache_in, f32[2,256]{1,0:T(2,128)} %get-tuple-element.8.first_in), custom_call_target="tpu_custom_call" | custom-call | tf_op jit(solution)/shard_map/hand_over/pallas_call | solution.py:695

commit v4 on v3

--- a/solution.py
+++ b/solution.py
@@ -16,6 +16,7 @@
 KC = 512
 D = 4096
 PAD = 16
+BLOCK = 64
 HE = E // 2
 ROWS = E + HE + PAD
 PIECES = ((0, 112), (112, 96))
@@ -142,16 +143,16 @@
     for cp in wcopies:
         cp.start()
 
-    wbd[...] = jnp.concatenate(
-        [wb_ref[...].astype(F32), wd_ref[...].astype(F32), jnp.zeros((PAD - 4, D), F32)], axis=0
-    ).astype(BF)
-
     barrier = pltpu.get_barrier_semaphore()
     partners = [{"y": yu}, {"y": yd}, {"c": other}]
     partners += [{"z": z_at(d)} for d in (1, -1, 2, -2)]
     partners += [{"x": lax.rem(x + d, NX)} for d in (1, 2, 3)]
     for p in partners:
         pl.semaphore_signal(barrier, inc=1, device_id=p, device_id_type=MESH)
+    small_rows = jnp.concatenate(
+        [wb_ref[...].astype(F32), wd_ref[...].astype(F32), jnp.zeros((PAD - 4, D), F32)], axis=0
+    )
+    wbd[...] = small_rows.T.astype(BF)
     pl.semaphore_wait(barrier, len(partners))
 
     def ycopy(s, half, direction):
@@ -223,44 +224,46 @@
         yarrive(s, 1, 1).wait_recv()
         fcopy(s, 1).start()
 
-    def finish_near(s):
+    def near_start(s):
         yarrive(s, 1, 0).wait_recv()
         pcopy(s, 1, c).start()
         yarrive(s, 0, 1).wait_recv()
         pcopy(s, 2, c).start()
+
+    def near_end(s):
         for k in range(3):
             pcopy(s, k, other).wait_recv()
 
-    def finish_far(s):
+    def far_start(s):
         farrive(s, 0).wait_recv()
         farrive(s, 1).wait_recv()
         pcopy(s, 3, c).start()
+
+    def far_end(s):
         pcopy(s, 3, other).wait_recv()
 
     it = lax.broadcasted_iota(jnp.int32, (L, L), 0)
     js = lax.broadcasted_iota(jnp.int32, (L, L), 1)
     lower = it >= js
-    strict = it > js
+    bt = lax.broadcasted_iota(jnp.int32, (BLOCK, BLOCK), 0)
+    bs = lax.broadcasted_iota(jnp.int32, (BLOCK, BLOCK), 1)
 
     def project(s, which):
         for i in which:
             pj[s, i] = dot(xbuf[s], wbuf[i]).astype(BF)
 
-    def small(s):
-        return dot_nt(xbuf[s], wbd[...])
-
     def chip(yy):
         return pl.ds(pl.multiple_of(yy * NC * KC, NC * KC), NC * KC)
 
     def near(s):
         for n, i in enumerate((1, 2)):
             acc[n] = sum(dot(xbuf[s, :, chip(q)], wbuf[i, chip(q), :]) for q in (y, yd, yu))
-        return sum(dot_nt(xbuf[s, :, chip(q)], wbd[:, chip(q)]) for q in (y, yd, yu))
+        return sum(dot(xbuf[s, :, chip(q)], wbd[chip(q), :]) for q in (y, yd, yu))
 
     def far(s, part):
         for n, i in enumerate((1, 2)):
             pj[s, i] = (acc[n] + dot(xbuf[s, :, chip(yf)], wbuf[i, chip(yf), :])).astype(BF)
-        return part + dot_nt(xbuf[s, :, chip(yf)], wbd[:, chip(yf)])
+        return part + dot(xbuf[s, :, chip(yf)], wbd[chip(yf), :])
 
     heads = range(2)
 
@@ -271,7 +274,7 @@
     def head_of(s, i, h):
         return pj[s, i, :, h * E : (h + 1) * E]
 
-    def chain_terms(s, bd):
+    def chain_terms(s, bd, between):
         lane = lax.broadcasted_iota(jnp.int32, (L, PAD), 1)
         bias = jnp.where(lane == 0, bias_ref[0], jnp.where(lane == 1, bias_ref[1], 0.0))
         rate = jnp.where(lane == 2, rate_ref[0], jnp.where(lane == 3, rate_ref[1], 0.0))
@@ -291,40 +294,65 @@
             0.0,
         ).astype(BF)
         rows = sum(dot_nt(eye, part) for part in split3(pack))
-        amats, cumc, betac = [], [], []
+        cumc = [cum[:, 2 + h : 3 + h] for h in heads]
+        betac = [beta[:, h : h + 1] for h in heads]
+
+        def corner(h, top, count, left):
+            span = slice(top, top + count)
+            kk = dot_nt(ks[h][span], ks[h][left : left + BLOCK])
+            gap = cumc[h][span] - rows[2 + h : 3 + h, left : left + BLOCK]
+            if top == left:
+                gap = jnp.where(bt > bs, gap, 0.0)
+            value = kk * (betac[h] * rk[h])[span] * jnp.exp(gap) * rows[h : h + 1, left : left + BLOCK]
+            return jnp.where(bt > bs, value, 0.0) if top == left else value
+
+        def level_mask(bit):
+            return ((bt >> (bit + 1)) == (bs >> (bit + 1))) & ((bt >> bit) != (bs >> bit))
+
+        diag = [corner(h, BLOCK * n, BLOCK, BLOCK * n) for h in heads for n in range(3)]
+        m = level_mask(0)
+        invs = [-jnp.where(m, a, 0.0) for a in diag]
+        for bit in range(1, 6):
+            m = level_mask(bit)
+            halfway = []
+            for a, inv in zip(diag, invs):
+                off = jnp.where(m, a, 0.0)
+                halfway.append(off + dot(off.astype(BF), inv.astype(BF)))
+            invs = [
+                inv - yy - dot(inv.astype(BF), yy.astype(BF)) for inv, yy in zip(invs, halfway)
+            ]
+        invs = [inv.astype(BF) for inv in invs]
+        between()
+        rhs, sols_of = [], [[], []]
         for h in heads:
-            cc = cum[:, 2 + h : 3 + h]
-            bc = beta[:, h : h + 1]
-            cumc.append(cc)
-            betac.append(bc)
-            rrow = rows[h : h + 1, :]
-            crow = rows[2 + h : 3 + h, :]
-            decay = jnp.exp(jnp.where(lower, cc - crow, 0.0)) * rrow
-            kk = dot_nt(ks[h], ks[h])
-            amats.append(jnp.where(strict, kk * (bc * rk[h]) * decay, 0.0))
-
-        def level_mask(bit):
-            return ((it >> (bit + 1)) == (js >> (bit + 1))) & ((it >> bit) != (js >> bit))
-
-        m0 = level_mask(0)
-        invs = [-jnp.where(m0, a, 0.0) for a in amats]
-        for bit in range(1, 8):
-            m = level_mask(bit)
+            kf = ks[h].astype(F32)
+            rhs.append(
+                jnp.concatenate(
+                    [
+                        kf * (betac[h] * rk[h] * jnp.exp(cumc[h])),
+                        vs[h].astype(F32) * betac[h],
+                    ],
+                    axis=1,
+                )
+            )
+        rest = rhs
+        for n in range(3):
             for h in heads:
-                off = jnp.where(m, amats[h], 0.0)
-                inv = invs[h]
-                ib = inv.astype(BF)
-                yy = off + dot(off.astype(BF), ib)
-                invs[h] = inv - yy - dot(ib, yy.astype(BF))
+                now = rest[h][:BLOCK]
+                sols_of[h].append((now + dot(invs[3 * h + n], now.astype(BF))).astype(BF))
+            if n < 2:
+                rest = [
+                    rest[h][BLOCK:]
+                    - dot(
+                        corner(h, BLOCK * (n + 1), L - BLOCK * (n + 1), BLOCK * n).astype(BF),
+                        sols_of[h][n],
+                    )
+                    for h in heads
+                ]
         for h in heads:
             b = 2 * s + h
             kf = ks[h].astype(F32)
-            ecum = jnp.exp(cumc[h])
-            rhs = jnp.concatenate(
-                [kf * (betac[h] * rk[h] * ecum), vs[h].astype(F32) * betac[h]], axis=1
-            )
-            sol = rhs + dot(invs[h].astype(BF), rhs.astype(BF))
-            sb = sol.astype(BF)
+            sb = jnp.concatenate(sols_of[h], axis=0)
             last = cumc[h][L - 1 : L, :]
             kd = kf * (rk[h] * jnp.exp(last - cumc[h]))
             rs = dot_tn(sb, kd.astype(BF)).astype(BF)
@@ -543,35 +571,38 @@
             norm = lax.rsqrt(jnp.mean(read * read, axis=1, keepdims=True) + 0.001)
             first_ref[s : s + 1, h * E : (h + 1) * E] = read * norm * gain
 
+    inner = []
     send_own(0)
     forward(0)
     send_own(1)
-    finish_near(0)
-    finish_far(0)
+    near_start(0)
+    near_end(0)
+    far_start(0)
     for cp in wcopies:
         cp.wait()
-    project(0, (1, 2))
+    part = near(0)
     forward(1)
-    kept0 = chain_terms(0, small(0))
+    far_end(0)
+    kept0 = chain_terms(0, far(0, part), lambda: near_start(1))
     xsend(0)
+    far_start(1)
+    near_end(1)
+    part = near(1)
+    far_end(1)
+    kept1 = chain_terms(1, far(1, part), lambda: inner.append(zsend(0)))
+    xsend(1)
     project(0, (0, 3))
     out_terms(0, *kept0)
-    finish_near(1)
-    part = near(1)
-    inner0 = zsend(0)
-    finish_far(1)
-    kept1 = chain_terms(1, far(1, part))
-    xsend(1)
+    project(1, (0, 3))
     zrelay(0)
-    project(1, (0, 3))
     out_terms(1, *kept1)
-    inner1 = zsend(1)
-    start_states(0, inner0)
+    inner.append(zsend(1))
     zrelay(1)
+    start_states(0, inner[0])
     final_parts(0)
+    start_states(1, inner[1])
+    final_parts(1)
     outputs(0)
-    start_states(1, inner1)
-    final_parts(1)
     last_parts(0)
     outputs(1)
     last_parts(1)
@@ -643,7 +674,7 @@
             pltpu.VMEM((4, D, 2 * E), BF),
             pltpu.VMEM((2, 4, L, 2 * E), BF),
             pltpu.VMEM((2, L, 2 * E), F32),
-            pltpu.VMEM((PAD, D), BF),
+            pltpu.VMEM((D, PAD), BF),
             pltpu.VMEM((4, L, E), F32),
             pltpu.VMEM((4, L, E), BF),
             pltpu.VMEM((4, L, 2 * E), BF),

time: 61.2 us -> 55.4 us (0.905); the launches traced: 61.1 us -> 54.3 us
  Pallas kernels: 60.4 us -> 53.6 us
    pallas_call x1, Pallas kernels: 58.8 us -> 52 us  [shards(): pl.pallas_call(kernel, out_shape=(jax.ShapeDtypeStruct((2, L, 2 * E), BF)...]
where the time goes in v4:
time: 55.4 us; the launch traced here: 54.3 us
  Pallas kernels  53.6 us (97%)
  between operations  0.65 us (1%)
    pallas_call x1, Pallas kernels, shards(): pl.pallas_call(kernel, out_shape=(jax.ShapeDtypeStruct((2, L, 2 * E), BF)...  52 us
    pallas_call x1, Pallas kernels, shards(): pl.pallas_call(hand_over, out_shape=tuple((jax.ShapeDtypeStruct(o.shape,...  1.63 us

profile of v4, /device:TPU:32, one launch (start us, length us, event | category | flops | bytes accessed | tf_op | source)
XLA Modules:
  0.0 54.3 jit_solution(7923746040646921506)
XLA Ops:
  0.6 52.0 %delta_all.1 = (bf16[2,192,256]{2,1,0:T(8,128)(2,1)}, bf16[2,2,4,128]{3,2,1,0:T(4,128)(2,1)}, f32[2,256]{1,0:T(2,128)}) custom-call(f32[2]{0:T(128)} %bias_ref.1, f32[2]{0:T(128)} %rate_ref.1, f32[2,2]{1,0:T(2,128)} %nbeta_ref.1, f32[2,2]{1,0:T(2,128)} %ndecay_ref.1, bf16[2,192,512]{2,1,0:T(8,128)(2,1)} %tok_ref.1, bf16[4096,256]{1,0:T(8,128)(2,1)} %wq_ref.1, ...), custom_call_target="tpu_custom_call" | custom-call | tf_op jit(solution)/shard_map/delta_all/pallas_call | solution.py:663
  52.6 1.6 %hand_over.1 = (bf16[2,192,256]{2,1,0:T(8,128)(2,1)}, bf16[2,2,4,128]{3,2,1,0:T(4,128)(2,1)}, f32[2,256]{1,0:T(2,128)}) custom-call(bf16[2,192,256]{2,1,0:T(8,128)(2,1)} %get-tuple-element.6.mixed_in, bf16[2,2,4,128]{3,2,1,0:T(4,128)(2,1)} %get-tuple-element.7.cache_in, f32[2,256]{1,0:T(2,128)} %get-tuple-element.8.first_in), custom_call_target="tpu_custom_call" | custom-call | tf_op jit(solution)/shard_map/hand_over/pallas_call | solution.py:726

commit v5 on v4

--- a/solution.py
+++ b/solution.py
@@ -149,10 +149,6 @@
     partners += [{"x": lax.rem(x + d, NX)} for d in (1, 2, 3)]
     for p in partners:
         pl.semaphore_signal(barrier, inc=1, device_id=p, device_id_type=MESH)
-    small_rows = jnp.concatenate(
-        [wb_ref[...].astype(F32), wd_ref[...].astype(F32), jnp.zeros((PAD - 4, D), F32)], axis=0
-    )
-    wbd[...] = small_rows.T.astype(BF)
     pl.semaphore_wait(barrier, len(partners))
 
     def ycopy(s, half, direction):
@@ -274,7 +270,7 @@
     def head_of(s, i, h):
         return pj[s, i, :, h * E : (h + 1) * E]
 
-    def chain_terms(s, bd, between):
+    def chain_terms(s, bd, between, ending):
         lane = lax.broadcasted_iota(jnp.int32, (L, PAD), 1)
         bias = jnp.where(lane == 0, bias_ref[0], jnp.where(lane == 1, bias_ref[1], 0.0))
         rate = jnp.where(lane == 2, rate_ref[0], jnp.where(lane == 3, rate_ref[1], 0.0))
@@ -349,6 +345,7 @@
                     )
                     for h in heads
                 ]
+        ending()
         for h in heads:
             b = 2 * s + h
             kf = ks[h].astype(F32)
@@ -496,6 +493,8 @@
         return pltpu.make_async_copy(side.at[s, t], sin.at[s, t], ss_sem.at[s, t])
 
     def start_states(s, inner):
+        m0, m10, m2 = inner
+        m210 = compose(m2, m10)
         zwait(s, 1, -1)
         behind = compose(zmap_if(s, -1), zmap_if(s, -2))
         early = apply_map(zmap_if(s, 2), zmap_if(s, 1)[1][E:])
@@ -503,12 +502,9 @@
         behind = compose(behind, zmap_if(s, -3))
         early = apply_map(zmap_if(s, -4), apply_map(zmap_if(s, 3), early))
         here = apply_map(behind, early)
-        m0, m10, m2 = inner
-        second = apply_map(m10, here)
-        ret[s, 0] = here.astype(BF)
-        ret[s, 1] = apply_map(m0, here).astype(BF)
-        ret[s, 2] = second.astype(BF)
-        ret[s, 3] = apply_map(m2, second).astype(BF)
+        ret_of = [here] + [apply_map(m, here) for m in (m0, m10, m210)]
+        for t in range(NX):
+            ret[s, t] = ret_of[t].astype(BF)
         spread(lambda t: rcopy(s, t, x), lambda t: rlocal(s, t))
 
     def unit(v):
@@ -573,6 +569,10 @@
 
     inner = []
     send_own(0)
+    small_rows = jnp.concatenate(
+        [wb_ref[...].astype(F32), wd_ref[...].astype(F32), jnp.zeros((PAD - 4, D), F32)], axis=0
+    )
+    wbd[...] = small_rows.T.astype(BF)
     forward(0)
     send_own(1)
     near_start(0)
@@ -583,13 +583,12 @@
     part = near(0)
     forward(1)
     far_end(0)
-    kept0 = chain_terms(0, far(0, part), lambda: near_start(1))
+    kept0 = chain_terms(0, far(0, part), lambda: near_start(1), lambda: far_start(1))
     xsend(0)
-    far_start(1)
     near_end(1)
     part = near(1)
     far_end(1)
-    kept1 = chain_terms(1, far(1, part), lambda: inner.append(zsend(0)))
+    kept1 = chain_terms(1, far(1, part), lambda: inner.append(zsend(0)), lambda: None)
     xsend(1)
     project(0, (0, 3))
     out_terms(0, *kept0)

time: 55.4 us -> 55.4 us (level); the launches traced: 54.3 us -> 55 us
  Pallas kernels: 53.6 us -> 54.4 us
    pallas_call x1, Pallas kernels: 52 us -> 52.8 us  [shards(): pl.pallas_call(kernel, out_shape=(jax.ShapeDtypeStruct((2, L, 2 * E), BF)...]
where the time goes in v5:
time: 55.4 us; the launch traced here: 55 us
  Pallas kernels  54.4 us (98%)
  between operations  0.65 us (1%)
    pallas_call x1, Pallas kernels, shards(): pl.pallas_call(kernel, out_shape=(jax.ShapeDtypeStruct((2, L, 2 * E), BF)...  52.8 us
    pallas_call x1, Pallas kernels, shards(): pl.pallas_call(hand_over, out_shape=tuple((jax.ShapeDtypeStruct(o.shape,...  1.63 us

profile of v5, /device:TPU:32, one launch (start us, length us, event | category | flops | bytes accessed | tf_op | source)
XLA Modules:
  0.0 55.0 jit_solution(14570041885687011503)
XLA Ops:
  0.6 52.8 %delta_all.1 = (bf16[2,192,256]{2,1,0:T(8,128)(2,1)}, bf16[2,2,4,128]{3,2,1,0:T(4,128)(2,1)}, f32[2,256]{1,0:T(2,128)}) custom-call(f32[2]{0:T(128)} %bias_ref.1, f32[2]{0:T(128)} %rate_ref.1, f32[2,2]{1,0:T(2,128)} %nbeta_ref.1, f32[2,2]{1,0:T(2,128)} %ndecay_ref.1, bf16[2,192,512]{2,1,0:T(8,128)(2,1)} %tok_ref.1, bf16[4096,256]{1,0:T(8,128)(2,1)} %wq_ref.1, ...), custom_call_target="tpu_custom_call" | custom-call | tf_op jit(solution)/shard_map/delta_all/pallas_call | solution.py:662
  53.4 1.6 %hand_over.1 = (bf16[2,192,256]{2,1,0:T(8,128)(2,1)}, bf16[2,2,4,128]{3,2,1,0:T(4,128)(2,1)}, f32[2,256]{1,0:T(2,128)}) custom-call(bf16[2,192,256]{2,1,0:T(8,128)(2,1)} %get-tuple-element.6.mixed_in, bf16[2,2,4,128]{3,2,1,0:T(4,128)(2,1)} %get-tuple-element.7.cache_in, f32[2,256]{1,0:T(2,128)} %get-tuple-element.8.first_in), custom_call_target="tpu_custom_call" | custom-call | tf_op jit(solution)/shard_map/hand_over/pallas_call | solution.py:725

commit v6 on v5

--- a/solution.py
+++ b/solution.py
@@ -632,10 +632,13 @@
                     zcopy(s, z_at(-2 * d), piece, 2 * d, 4).wait_send()
 
 
-def hand_over(mixed_in, cache_in, first_in, mixed_out, cache_out, first_out):
-    mixed_out[...] = mixed_in[...]
-    cache_out[...] = cache_in[...]
-    first_out[...] = first_in[...]
+def hand_over(mixed_in, cache_in, first_in, mixed_out, cache_out, first_out, sems):
+    pairs = ((mixed_in, mixed_out), (cache_in, cache_out), (first_in, first_out))
+    copies = [pltpu.make_async_copy(a, b, sems.at[n]) for n, (a, b) in enumerate(pairs)]
+    for cp in copies:
+        cp.start()
+    for cp in copies:
+        cp.wait()
 
 
 def shards(
@@ -725,8 +728,9 @@
     return pl.pallas_call(
         hand_over,
         out_shape=tuple(jax.ShapeDtypeStruct(o.shape, o.dtype) for o in out),
-        in_specs=[vmem] * 3,
+        in_specs=[hbm] * 3,
         out_specs=(vmem,) * 3,
+        scratch_shapes=[dma((3,))],
         name="hand_over",
     )(*out)
 

time: 55.4 us -> 55.4 us (level)
  no operation moved by 1% of the time
where the time goes in v6:
time: 55.4 us; the launch traced here: 55 us
  Pallas kernels  54.4 us (98%)
  between operations  0.65 us (1%)
    pallas_call x1, Pallas kernels, shards(): pl.pallas_call(kernel, out_shape=(jax.ShapeDtypeStruct((2, L, 2 * E), BF)...  52.8 us
    pallas_call x1, Pallas kernels, shards(): pl.pallas_call(hand_over, out_shape=tuple((jax.ShapeDtypeStruct(o.shape,...  1.64 us

profile of v6, /device:TPU:32, one launch (start us, length us, event | category | flops | bytes accessed | tf_op | source)
XLA Modules:
  0.0 55.0 jit_solution(4019805249411006703)
XLA Ops:
  0.6 52.8 %delta_all.1 = (bf16[2,192,256]{2,1,0:T(8,128)(2,1)}, bf16[2,2,4,128]{3,2,1,0:T(4,128)(2,1)}, f32[2,256]{1,0:T(2,128)}) custom-call(f32[2]{0:T(128)} %bias_ref.1, f32[2]{0:T(128)} %rate_ref.1, f32[2,2]{1,0:T(2,128)} %nbeta_ref.1, f32[2,2]{1,0:T(2,128)} %ndecay_ref.1, bf16[2,192,512]{2,1,0:T(8,128)(2,1)} %tok_ref.1, bf16[4096,256]{1,0:T(8,128)(2,1)} %wq_ref.1, ...), custom_call_target="tpu_custom_call" | custom-call | tf_op jit(solution)/shard_map/delta_all/pallas_call | solution.py:665
  53.4 1.6 %hand_over.1 = (bf16[2,192,256]{2,1,0:T(8,128)(2,1)}, bf16[2,2,4,128]{3,2,1,0:T(4,128)(2,1)}, f32[2,256]{1,0:T(2,128)}) custom-call(bf16[2,192,256]{2,1,0:T(8,128)(2,1)} %get-tuple-element.6.mixed_in, bf16[2,2,4,128]{3,2,1,0:T(4,128)(2,1)} %get-tuple-element.7.cache_in, f32[2,256]{1,0:T(2,128)} %get-tuple-element.8.first_in), custom_call_target="tpu_custom_call" | custom-call | tf_op jit(solution)/shard_map/hand_over/pallas_call | solution.py:728
